TPU v7x, 128 devices: a whole 4x4x4 slice. The times are simulated.
128 devices in a mesh: rep: 2 (over z_hi), fs: 32 (over z_lo, y, x), tp: 2 (over core).
Axes of the slice: x: 4, y: 4, z: 4 (z_hi: 2, z_lo: 2; z = z_hi * 2 + z_lo), core: 2. Of those that a mesh axis runs over, the one named last changes fastest.
Arguments:
- tokens: bfloat16 [32768, 2048], P(('rep', 'fs'), 'tp'), may hold values from -6 to 6
- mix_gain: float32 [2048], replicated, may hold values from 0.1 to 1.9
- lru_input: float32 [2048, 2048], P('fs', 'tp'), may hold values from -0.125 to 0.125
- lru_gate: float32 [2048, 2048], P('fs', 'tp'), may hold values from -0.125 to 0.125
- lru_input_scale: float32 [2048], P('tp'), may hold values from 0.5 to 2
- lru_gate_scale: float32 [2048], P('tp'), may hold values from 0.5 to 2
- conv_weight: float32 [4, 2048], P(None, 'tp'), may hold values from -3 to 3
- recur_gate: float32 [32, 64, 64], P('tp'), may hold values from -0.75 to 0.75
- input_gate: float32 [32, 64, 64], P('tp'), may hold values from -0.75 to 0.75
- decay_rate: float32 [2048], P('tp'), may hold values from 3.5 to 9
- extra_decay: float32 [32768], P(('rep', 'fs')), may hold values from 0.0003 to 2.1
- lru_output: float32 [2048, 2048], P('tp', 'fs'), may hold values from -0.125 to 0.125
- lru_output_scale: float32 [2048], replicated, may hold values from 0.5 to 2
- ffn_gain: float32 [2048], replicated, may hold values from 0.1 to 1.9
- ffn_gate: float32 [2048, 2816], P('fs', 'tp'), may hold values from -0.125 to 0.125
- ffn_up: float32 [2048, 2816], P('fs', 'tp'), may hold values from -0.125 to 0.125
- ffn_gate_scale: float32 [2816], P('tp'), may hold values from 0.5 to 2
- ffn_up_scale: float32 [2816], P('tp'), may hold values from 0.5 to 2
- ffn_down: float32 [2816, 2048], P('tp', 'fs'), may hold values from -0.109375 to 0.109375
- ffn_down_scale: float32 [2048], replicated, may hold values from 0.5 to 2
Outputs:
- layer_out: bfloat16 [32768, 2048], P(('rep', 'fs'), 'tp')
All inputs are finite; a program needn't handle non-finite values.
Results may differ from a plain program's by a relative error of at most 0.02.
Values may be sent and summed in bfloat16 or wider, within the bound.
A program may use at most 192 MiB of HBM per device.

v0:
```python
import functools

import jax
import jax.numpy as jnp
from jax import lax
from jax.experimental import pallas as pl
from jax.experimental.pallas import tpu as pltpu
from jax.sharding import PartitionSpec as P

EPS = 1e-06
RATE = 8.0
LANES = 128
MESH = pl.DeviceIdType.MESH
GROUPS = (4, 4, 3)
f32, bf16 = jnp.float32, jnp.bfloat16


def sigmoid(v):
    return 1.0 / (1.0 + jnp.exp(-v))


def layer_kernel(
    chunks, tok, piece, mix_gain, in_scale, gt_scale, conv_ref, map_ref, rate_ref, extra_ref,
    out_scale, ffn_gain, fg_scale, fu_scale, dn_scale, out_ref,
    W, X, N, BI, ST, GA, SB, RB, RB2, H, PS,
    send_sem, recv_sem, tp_send, tp_recv, own_sem,
):
    rep, fs, tp = lax.axis_index("rep"), lax.axis_index("fs"), lax.axis_index("tp")
    zl, y, x = fs // 16, (fs // 4) % 4, fs % 4
    rows, half = tok.shape
    up = lambda v: lax.rem(v + 1, 4)
    dn = lambda v: lax.rem(v + 3, 4)
    xl, xr, yl, yr = dn(x), up(x), dn(y), up(y)
    other = 1 - tp
    to_x = lambda v: (rep, zl * 16 + y * 4 + v, tp)
    to_y = lambda v: (rep, zl * 16 + v * 4 + x, tp)
    z_other = (1 - zl) * 16 + y * 4 + x
    z_next = (jnp.where(zl == 0, rep, 1 - rep), z_other, tp)
    z_prev = (jnp.where(zl == 0, 1 - rep, rep), z_other, tp)
    partner = (rep, fs, other)

    barrier = pltpu.get_barrier_semaphore()
    for peer in (to_x(xl), to_x(xr), to_y(yl), to_y(yr), z_next, z_prev, partner):
        pl.semaphore_signal(barrier, inc=1, device_id=peer, device_id_type=MESH)

    own = []
    for k, (start, width) in enumerate(chunks):
        cols = pl.ds(start, width)
        c = pltpu.make_async_copy(piece.at[:, cols], W.at[zl, y, x, :, cols], own_sem.at[k])
        c.start()
        own.append(c)
    keep = pltpu.make_async_copy(tok, X.at[tp], own_sem.at[len(chunks)])
    keep.start()

    def remote(src, dst, target, ssem, rsem):
        return pltpu.make_async_remote_copy(
            src_ref=src, dst_ref=dst, send_sem=ssem, recv_sem=rsem,
            device_id=target, device_id_type=MESH,
        )

    A, B = pl.ds(0, 32), pl.ds(32, 32)
    every = slice(None)

    def plan(k):
        cols = pl.ds(*chunks[k])
        at = lambda a, b, c, r: W.at[a, b, c, r, cols]
        return [
            [(at(zl, y, x, A), z_next), (at(zl, y, x, B), z_prev)],
            [
                (at(every, y, x, A), to_x(xr)), (at(every, y, x, A), to_x(xl)),
                (at(every, y, x, B), to_y(yr)), (at(every, y, x, B), to_y(yl)),
            ],
            [
                (at(0, y, xl, A), to_x(xr)), (at(1, y, xr, A), to_x(xl)),
                (at(0, yl, x, B), to_y(yr)), (at(1, yr, x, B), to_y(yl)),
            ],
            [
                (at(every, y, every, A), to_y(yr)), (at(every, y, every, A), to_y(yl)),
                (at(every, every, x, B), to_x(xr)), (at(every, every, x, B), to_x(xl)),
            ],
            [
                (at(0, yl, every, A), to_y(yr)), (at(1, yr, every, A), to_y(yl)),
                (at(0, every, xl, B), to_x(xr)), (at(1, every, xr, B), to_x(xl)),
            ],
        ]

    flights = {}

    def issue(k, s):
        if k >= len(chunks):
            return
        if s == 0:
            own[k].wait()
        else:
            land(k, s - 1)
        base = sum(len(p) for p in plan(k)[:s])
        flights[k, s] = []
        for i, (ref, target) in enumerate(plan(k)[s]):
            c = remote(ref, ref, target, send_sem.at[k, base + i], recv_sem.at[k, base + i])
            c.start()
            flights[k, s].append(c)

    def land(k, s):
        for c in flights[k, s]:
            c.wait_recv()

    pl.semaphore_wait(barrier, 7)
    swap_tok = remote(tok, X.at[tp], partner, tp_send.at[0], tp_recv.at[0])
    swap_tok.start()
    for k in range(len(chunks)):
        issue(k, 0)
    issue(0, 1)
    issue(1, 1)
    keep.wait()
    swap_tok.wait_recv()

    def norm_rows(gain):
        step = 64

        def body(i, carry):
            r = pl.ds(pl.multiple_of(i * step, step), step)
            lo, hi = X[0, r, :].astype(f32), X[1, r, :].astype(f32)
            total = jnp.sum(lo * lo, axis=-1, keepdims=True) + jnp.sum(
                hi * hi, axis=-1, keepdims=True
            )
            scale = lax.rsqrt(total / (2 * half) + EPS)
            N[r, :half] = (lo * scale * gain[:, :half]).astype(bf16)
            N[r, half:] = (hi * scale * gain[:, half:]).astype(bf16)
            return carry

        lax.fori_loop(0, rows // step, body, 0)

    def wide(start, width):
        return W[:, :, :, :, pl.ds(start, width)].reshape(2 * half, width)

    def dot(a, b):
        return jnp.dot(a, b, preferred_element_type=f32)

    def dot_t(a, b):
        return lax.dot_general(a, b, (((1,), (1,)), ((), ())), preferred_element_type=f32)

    def branch_in():
        def body(i, carry):
            c = pl.multiple_of(i * 256, 256)
            BI[:, pl.ds(c, 256)] = (
                dot(N[...], wide(c, 256)) * in_scale[:, pl.ds(c, 256)]
            ).astype(bf16)
            return carry

        lax.fori_loop(0, half // 256, body, 0)

    def scan_block(i, carry):
        cols = pl.ds(pl.multiple_of(i * LANES, LANES), LANES)
        length = rows
        taps = conv_ref.shape[0]
        values = BI[:, cols].astype(f32)
        weights = conv_ref[:, cols]
        row = lax.broadcasted_iota(jnp.int32, values.shape, 0)
        conv = weights[taps - 1 : taps, :] * values
        for back in range(1, taps):
            moved = jnp.where(row >= back, pltpu.roll(values, back, 0), 0.0)
            conv = conv + weights[taps - 1 - back : taps - back, :] * moved
        mapped = jnp.dot(
            conv, map_ref[i], preferred_element_type=f32, precision=lax.Precision.HIGHEST
        )
        recur = sigmoid(mapped[:, :LANES])
        ingate = sigmoid(mapped[:, LANES:])
        log_rate = rate_ref[:, cols] * recur - extra_ref[...]
        a = jnp.exp(log_rate)
        u = -2.0 * log_rate
        series = u * (1 - u / 2 * (1 - u / 3 * (1 - u / 4 * (1 - u / 5 * (1 - u / 6)))))
        b = jnp.sqrt(jnp.where(u < 0.25, series, 1.0 - jnp.exp(-u))) * (ingate * conv)
        inner = row % 8
        for s in (1, 2, 4):
            live = inner >= s
            b = jnp.where(live, a * pltpu.roll(b, s, 0) + b, b)
            a = jnp.where(live, a * pltpu.roll(a, s, 0), a)
        groups = length // 8
        last_a = a.reshape(groups, 8, LANES)
        last_b = b.reshape(groups, 8, LANES)
        ca = jnp.broadcast_to(last_a[:, 7:8, :], last_a.shape).reshape(length, LANES)
        cb = jnp.broadcast_to(last_b[:, 7:8, :], last_b.shape).reshape(length, LANES)
        s = 8
        while s < length:
            cb_new = ca[s:] * cb[:-s] + cb[s:]
            ca_new = ca[s:] * ca[:-s]
            cb = jnp.concatenate([cb[:s], cb_new], axis=0)
            ca = jnp.concatenate([ca[:s], ca_new], axis=0)
            s *= 2
        ST[:, cols] = jnp.concatenate([b[:8], a[8:] * cb[:-8] + b[8:]], axis=0)
        return carry

    def gate_block(i, carry):
        c = pl.multiple_of(i * 256, 256)
        cols = pl.ds(c, 256)
        acc = dot(N[...], wide(pl.multiple_of(half + c, 256), 256)) * gt_scale[:, cols]
        g = acc.astype(bf16).astype(f32)
        gelu = 0.5 * g * (1.0 + jnp.tanh(0.7978845608028654 * (g + 0.044715 * g * g * g)))
        GA[:, cols] = (ST[:, cols] * gelu).astype(bf16)
        return carry

    def rows_of(block, j, start, width):
        return W[block, j, :, :, pl.ds(start, width)].reshape(256, width)

    def mixer_out():
        def send_body(j, carry):
            cols = pl.ds(pl.multiple_of(j * 256, 256), 256)
            SB[:, cols] = dot_t(GA[...], rows_of(other, j, 2 * half, half)).astype(bf16)
            return carry

        def mine_body(j, carry):
            cols = pl.ds(pl.multiple_of(j * 256, 256), 256)
            PS[0, :, cols] = dot_t(GA[...], rows_of(tp, j, 2 * half, half))
            return carry

        lax.fori_loop(0, 4, send_body, 0)
        swap = remote(SB, RB, partner, tp_send.at[1], tp_recv.at[1])
        swap.start()
        lax.fori_loop(0, 4, mine_body, 0)
        swap.wait_recv()

        def mixed_body(i, carry):
            r = pl.ds(pl.multiple_of(i * 64, 64), 64)
            total = PS[0, r, :] + RB[r, :].astype(f32)
            X[tp, r, :] = (tok[r, :].astype(f32) + total * out_scale[...]).astype(bf16)
            return carry

        lax.fori_loop(0, rows // 64, mixed_body, 0)
        swap.wait_send()
        share = remote(X.at[tp], X.at[tp], partner, tp_send.at[2], tp_recv.at[2])
        share.start()
        share.wait()
        norm_rows(ffn_gain)

    def hidden_tile(unit, start):
        cols = pl.ds(pl.multiple_of(unit * LANES, LANES), LANES)
        both = dot(N[...], wide(start, 256))
        gate = both[:, :LANES] * fg_scale[:, cols]
        lift = both[:, LANES:] * fu_scale[:, cols]
        H[:, cols] = (gate / (1.0 + jnp.exp(-gate)) * lift).astype(bf16)

    def ffn(g):
        first, count = sum(GROUPS[:g]), GROUPS[g]
        start = 3 * half + first * 3 * LANES
        lax.fori_loop(
            0, count,
            lambda t, c: (hidden_tile(first + t, pl.multiple_of(start + t * 256, 128)), c)[1], 0,
        )
        down = start + count * 256
        acts = lambda: H[:, first * LANES : (first + count) * LANES]

        def part(slot, block, j):
            cols = pl.ds(pl.multiple_of(j * 256, 256), 256)
            v = dot_t(acts(), rows_of(block, j, down, count * LANES))
            if g > 0:
                v = PS[slot, :, cols] + v
            return cols, v

        last = g == len(GROUPS) - 1

        def away(j, carry):
            cols, v = part(1, other, j)
            if last:
                SB[:, cols] = v.astype(bf16)
            else:
                PS[1, :, cols] = v
            return carry

        def home(j, carry):
            cols, v = part(0, tp, j)
            PS[0, :, cols] = v
            return carry

        lax.fori_loop(0, 4, away, 0)
        if last:
            swap = remote(SB, RB2, partner, tp_send.at[3], tp_recv.at[3])
            swap.start()
        lax.fori_loop(0, 4, home, 0)
        if last:
            swap.wait()

            def final(i, carry):
                r = pl.ds(pl.multiple_of(i * 64, 64), 64)
                total = PS[0, r, :] + RB2[r, :].astype(f32)
                out_ref[r, :] = (X[tp, r, :].astype(f32) + total * dn_scale[...]).astype(bf16)
                return carry

            lax.fori_loop(0, rows // 64, final, 0)

    issue(0, 2)
    norm_rows(mix_gain)
    issue(1, 2)
    issue(0, 3)
    issue(2, 1)
    issue(0, 4)
    issue(1, 3)
    issue(2, 2)
    issue(3, 1)
    land(0, 4)
    branch_in()
    lax.fori_loop(0, 2, scan_block, 0)
    issue(1, 4)
    issue(2, 3)
    issue(3, 2)
    issue(4, 1)
    lax.fori_loop(2, 5, scan_block, 0)
    land(1, 4)
    issue(2, 4)
    issue(3, 3)
    issue(4, 2)
    issue(5, 1)
    lax.fori_loop(5, 8, scan_block, 0)
    lax.fori_loop(0, 4, gate_block, 0)
    issue(3, 4)
    issue(4, 3)
    issue(5, 2)
    land(2, 4)
    mixer_out()
    issue(4, 4)
    issue(5, 3)
    land(3, 4)
    ffn(0)
    issue(5, 4)
    land(4, 4)
    ffn(1)
    land(5, 4)
    ffn(2)
    swap_tok.wait_send()
    for group in flights.values():
        for c in group:
            c.wait_send()


def local(*args):
    (
        tokens, mix_gain, lru_input, lru_gate, lru_input_scale, lru_gate_scale, conv_weight,
        recur_gate, input_gate, decay_rate, extra_decay, lru_output, lru_output_scale, ffn_gain,
        ffn_gate, ffn_up, ffn_gate_scale, ffn_up_scale, ffn_down, ffn_down_scale,
    ) = args
    tp = lax.axis_index("tp")
    rows, half = tokens.shape
    units = ffn_gate.shape[1] // LANES

    out_t = lru_output.astype(bf16).T
    down_t = ffn_down.astype(bf16).T
    gate16, up16 = ffn_gate.astype(bf16), ffn_up.astype(bf16)
    parts = [lru_input.astype(bf16), lru_gate.astype(bf16), out_t]
    chunks = [(0, half), (half, half), (2 * half, half)]
    first = 0
    for count in GROUPS:
        for t in range(first, first + count):
            cut = slice(t * LANES, (t + 1) * LANES)
            parts += [gate16[:, cut], up16[:, cut]]
        parts.append(down_t[:, first * LANES : (first + count) * LANES])
        chunks.append((3 * half + first * 3 * LANES, count * 3 * LANES))
        first += count
    assert first == units
    piece = jnp.concatenate(parts, axis=1)
    width = piece.shape[1]

    per = LANES // recur_gate.shape[1]
    groups = recur_gate.shape[0] // per

    def block_diag(blocks):
        tall = blocks.reshape(groups, LANES, blocks.shape[2])
        both = jnp.concatenate([tall] * per, axis=2)
        r = lax.broadcasted_iota(jnp.int32, both.shape, 1) // blocks.shape[1]
        c = lax.broadcasted_iota(jnp.int32, both.shape, 2) // blocks.shape[2]
        return jnp.where(r == c, both, 0.0)

    maps = jnp.concatenate([block_diag(recur_gate), block_diag(input_gate)], axis=2)
    rate = (-RATE * jax.nn.softplus(-decay_rate))[None, :]
    mine = lambda v: lax.dynamic_slice_in_dim(v, tp * half, half)[None, :]
    n = len(chunks)
    vmem = pl.BlockSpec(memory_space=pltpu.VMEM)
    return pl.pallas_call(
        functools.partial(layer_kernel, tuple(chunks)),
        out_shape=jax.ShapeDtypeStruct((rows, half), bf16),
        in_specs=[vmem, pl.BlockSpec(memory_space=pl.ANY)] + [vmem] * 12,
        out_specs=vmem,
        scratch_shapes=[
            pltpu.VMEM((2, 4, 4, 64, width), bf16),
            pltpu.VMEM((2, rows, half), bf16),
            pltpu.VMEM((rows, 2 * half), bf16),
            pltpu.VMEM((rows, half), bf16),
            pltpu.VMEM((rows, half), f32),
            pltpu.VMEM((rows, half), bf16),
            pltpu.VMEM((rows, half), bf16),
            pltpu.VMEM((rows, half), bf16),
            pltpu.VMEM((rows, half), bf16),
            pltpu.VMEM((rows, units * LANES), bf16),
            pltpu.VMEM((2, rows, half), f32),
            pltpu.SemaphoreType.DMA((n, 18)),
            pltpu.SemaphoreType.DMA((n, 18)),
            pltpu.SemaphoreType.DMA((4,)),
            pltpu.SemaphoreType.DMA((4,)),
            pltpu.SemaphoreType.DMA((n + 1,)),
        ],
        compiler_params=pltpu.CompilerParams(
            collective_id=0, has_side_effects=True, vmem_limit_bytes=67043328
        ),
        name="layer",
    )(
        tokens, piece, mix_gain[None, :], lru_input_scale[None, :], lru_gate_scale[None, :],
        conv_weight, maps, rate, extra_decay[:, None], mine(lru_output_scale), ffn_gain[None, :],
        ffn_gate_scale[None, :], ffn_up_scale[None, :], mine(ffn_down_scale),
    )


def solution(mesh):
    in_specs = (
        P(("rep", "fs"), "tp"), P(), P("fs", "tp"), P("fs", "tp"), P("tp"), P("tp"),
        P(None, "tp"), P("tp", None, None), P("tp", None, None), P("tp"), P(("rep", "fs")),
        P("tp", "fs"), P(), P(), P("fs", "tp"), P("fs", "tp"), P("tp"), P("tp"), P("tp", "fs"),
        P(),
    )
    return jax.shard_map(
        local, mesh=mesh, in_specs=in_specs, out_specs=P(("rep", "fs"), "tp"), check_vma=False
    )
```

profile of v0, /device:TPU:1, one launch (start us, length us, event | category | flops | bytes accessed | tf_op | source)
XLA Modules:
  0.0 208.7 jit_solution(11022082993176344531)
XLA Ops:
  0.0 1.3 fusion
  1.4 1.3 dynamic_slice.6
  2.6 1.3 dynamic_slice.7
  3.9 1.3 broadcast_in_dim.43.fg_scale
  5.2 1.3 broadcast_in_dim.44.fu_scale
  6.5 1.0 convert_element_type.21
  7.6 0.9 copy-done.3
  8.5 0.7 copy-done.7
  9.2 0.9 copy.21.extra_ref
  10.1 0.7 convert_dynamic-update-slice_fusion.1
  11.1 0.7 convert_dynamic-update-slice_fusion
  12.1 0.7 bitcast_dynamic-update-slice_fusion
  12.8 0.6 constant_dynamic-update-slice_fusion.22
  14.0 0.6 constant_dynamic-update-slice_fusion.20
  15.8 0.6 constant_dynamic-update-slice_fusion.17
  16.5 0.6 constant_dynamic-update-slice_fusion.16
  17.7 0.6 slice_dynamic-update-slice_fusion.1
  20.1 0.6 constant_dynamic-update-slice_fusion.11
  21.3 0.6 constant_dynamic-update-slice_fusion.9
  23.1 0.6 slice_dynamic-update-slice_fusion
  27.4 0.7 constant_dynamic-update-slice_fusion.piece
  28.4 1.0 pad_maximum_fusion.map_ref
  29.5 177.0 %layer.1 = bf16[512,1024]{1,0:T(8,128)(2,1)} custom-call(bf16[512,1024]{1,0:T(8,128)(2,1)} %tok.1, bf16[64,7296]{1,0:T(8,128)(2,1)} %constant_dynamic-update-slice_fusion.piece, f32[1,2048]{1,0:T(1,128)} %bitcast.19, f32[1,1024]{1,0:T(1,128)} %bitcast.21, f32[1,1024]{1,0:T(1,128)} %bitcast.22, f32[4,1024]{1,0:T(4,128)} %conv_ref.1, ...), custom_call_target="tpu_custom_call" | custom-call | tf_op jit(solution)/shard_map/layer/pallas_call | solution.py:376
  206.4 2.3 %copy.50 = bf16[512,1024]{1,0:T(8,128)(2,1)} copy(bf16[512,1024]{1,0:T(8,128)(2,1)} %layer.1) | data formatting | bytes 2097152
  (35 shorter events, 10.8 us)
Async XLA Ops:
  0.0 7.5 %copy-start.2 = (f32[64,1408]{1,0:T(8,128)S(1)}, f32[64,1408]{1,0:T(8,128)}, u32[]{:S(2)}) copy-start(f32[64,1408]{1,0:T(8,128)} %param.35) | copy-start | bytes 1081348
  7.5 1.0 copy-start.3
  8.5 0.7 copy-start.7
  9.2 0.9 copy-start.4
  10.1 1.0 copy-start.5
  11.1 1.0 copy-start.6
  12.8 15.2 %copy-start.1 = (f32[16,64,64]{2,1,0:T(8,128)S(1)}, f32[16,64,64]{2,1,0:T(8,128)}, u32[]{:S(2)}) copy-start(f32[16,64,64]{2,1,0:T(8,128)} %param.28) | copy-start | bytes 786436
  13.4 14.6 %copy-start = (f32[16,64,64]{2,1,0:T(8,128)S(1)}, f32[16,64,64]{2,1,0:T(8,128)}, u32[]{:S(2)}) copy-start(f32[16,64,64]{2,1,0:T(8,128)} %param.27) | copy-start | bytes 786436
where the time goes:
time: 209 us
  Pallas kernels  177 us (85%)
  local copies, waits for them, and re-layouts  25.8 us (12%)
  other arithmetic  5.87 us (3%)
    pallas_call x1, Pallas kernels, local(): pl.pallas_call(functools.partial(layer_kernel, tuple(chunks)), out_shape=...  177 us
    unnamed x41, local copies, waits for them, and re-layouts  19.1 us

commit v1 on v0

--- a/solution.py
+++ b/solution.py
@@ -20,36 +20,40 @@
 
 
 def layer_kernel(
-    chunks, tok, piece, mix_gain, in_scale, gt_scale, conv_ref, map_ref, rate_ref, extra_ref,
+    chunks, tok, w_in, w_gate, w_out, w_fg, w_fu, w_dn,
+    mix_gain, in_scale, gt_scale, conv_ref, recur_ref, ingate_ref, decay_ref, extra_ref,
     out_scale, ffn_gain, fg_scale, fu_scale, dn_scale, out_ref,
-    W, X, N, BI, ST, GA, SB, RB, RB2, H, PS,
+    W, X, N, BI, ST, GA, SB, RB, RB2, H, PS, F1, F2, F3, F4, F5, F6, MAP, RATES, EX,
     send_sem, recv_sem, tp_send, tp_recv, own_sem,
 ):
     rep, fs, tp = lax.axis_index("rep"), lax.axis_index("fs"), lax.axis_index("tp")
     zl, y, x = fs // 16, (fs // 4) % 4, fs % 4
     rows, half = tok.shape
+    n = len(chunks)
     up = lambda v: lax.rem(v + 1, 4)
     dn = lambda v: lax.rem(v + 3, 4)
     xl, xr, yl, yr = dn(x), up(x), dn(y), up(y)
-    other = 1 - tp
+    other, away_zl = 1 - tp, 1 - zl
     to_x = lambda v: (rep, zl * 16 + y * 4 + v, tp)
     to_y = lambda v: (rep, zl * 16 + v * 4 + x, tp)
-    z_other = (1 - zl) * 16 + y * 4 + x
-    z_next = (jnp.where(zl == 0, rep, 1 - rep), z_other, tp)
-    z_prev = (jnp.where(zl == 0, 1 - rep, rep), z_other, tp)
+    z_other = away_zl * 16 + y * 4 + x
+    rep_next = jnp.where(zl == 0, rep, 1 - rep)
+    rep_prev = 1 - rep_next
+    z_next, z_prev = (rep_next, z_other, tp), (rep_prev, z_other, tp)
     partner = (rep, fs, other)
 
     barrier = pltpu.get_barrier_semaphore()
     for peer in (to_x(xl), to_x(xr), to_y(yl), to_y(yr), z_next, z_prev, partner):
         pl.semaphore_signal(barrier, inc=1, device_id=peer, device_id_type=MESH)
 
-    own = []
-    for k, (start, width) in enumerate(chunks):
-        cols = pl.ds(start, width)
-        c = pltpu.make_async_copy(piece.at[:, cols], W.at[zl, y, x, :, cols], own_sem.at[k])
+    loads = []
+    for i, (src, dst) in enumerate(
+        [(w_in, F1), (w_gate, F2), (w_out, F3), (w_fg, F4), (w_fu, F5), (w_dn, F6)]
+    ):
+        c = pltpu.make_async_copy(src, dst, own_sem.at[i])
         c.start()
-        own.append(c)
-    keep = pltpu.make_async_copy(tok, X.at[tp], own_sem.at[len(chunks)])
+        loads.append(c)
+    keep = pltpu.make_async_copy(tok, X.at[tp], own_sem.at[6])
     keep.start()
 
     def remote(src, dst, target, ssem, rsem):
@@ -60,57 +64,159 @@
 
     A, B = pl.ds(0, 32), pl.ds(32, 32)
     every = slice(None)
+    lo2, hi2 = pl.ds(0, 2), pl.ds(2, 2)
+    mine_rows = pl.ds(pl.multiple_of(rep * 32, 32), 32)
+    CA = pl.ds(pl.multiple_of(rep * 32, 16), 16)
+    CB = pl.ds(pl.multiple_of(rep * 32 + 16, 16), 16)
+    next_rows = pl.ds(pl.multiple_of(rep_next * 32, 32), 32)
+    prev_rows = pl.ds(pl.multiple_of(rep_prev * 32, 32), 32)
+    up_x, dn_x, up_y, dn_y = to_x(xr), to_x(xl), to_y(yr), to_y(yl)
+    needs = {
+        "z0": (), "s1": ("z0",), "s2": ("s1",), "s3a": ("s2",), "s3b": ("s2",), "s4": ("s3a",),
+        "c1": (), "c2": ("c1",), "c3": ("c2",), "c4": ("c3",), "c5a": ("c4",), "c5b": ("c4",),
+        "c6": ("c5a",),
+    }
 
     def plan(k):
-        cols = pl.ds(*chunks[k])
+        start, width, last = chunks[k]
+        cols, tail = pl.ds(start, width - last), pl.ds(start + width - last, last)
+        cut = (last // LANES + 1) // 2 * LANES
+        t1 = pl.ds(start + width - last, cut)
+        t2 = pl.ds(start + width - last + cut, last - cut)
         at = lambda a, b, c, r: W.at[a, b, c, r, cols]
-        return [
-            [(at(zl, y, x, A), z_next), (at(zl, y, x, B), z_prev)],
-            [
-                (at(every, y, x, A), to_x(xr)), (at(every, y, x, A), to_x(xl)),
-                (at(every, y, x, B), to_y(yr)), (at(every, y, x, B), to_y(yl)),
-            ],
-            [
-                (at(0, y, xl, A), to_x(xr)), (at(1, y, xr, A), to_x(xl)),
-                (at(0, yl, x, B), to_y(yr)), (at(1, yr, x, B), to_y(yl)),
-            ],
-            [
-                (at(every, y, every, A), to_y(yr)), (at(every, y, every, A), to_y(yl)),
-                (at(every, every, x, B), to_x(xr)), (at(every, every, x, B), to_x(xl)),
-            ],
-            [
-                (at(0, yl, every, A), to_y(yr)), (at(1, yr, every, A), to_y(yl)),
-                (at(0, every, xl, B), to_x(xr)), (at(1, every, xr, B), to_x(xl)),
-            ],
-        ]
-
-    flights = {}
-
-    def issue(k, s):
-        if k >= len(chunks):
+        ct = lambda a, b, c, r, t=tail: W.at[a, b, c, r, t]
+        return {
+            "z0": [(at(zl, y, x, A), z_next), (at(zl, y, x, B), z_prev)],
+            "s1": [
+                (at(every, y, x, A), up_x), (at(every, y, x, A), dn_x),
+                (at(every, y, x, B), up_y), (at(every, y, x, B), dn_y),
+            ],
+            "s2": [
+                (at(0, y, xl, A), up_x), (at(1, y, xr, A), dn_x),
+                (at(0, yl, x, B), up_y), (at(1, yr, x, B), dn_y),
+            ],
+            "s3a": [
+                (at(0, y, every, A), up_y), (at(1, y, every, A), dn_y),
+                (at(0, every, x, B), up_x), (at(1, every, x, B), dn_x),
+            ],
+            "s3b": [
+                (at(1, y, every, A), up_y), (at(0, y, every, A), dn_y),
+                (at(1, every, x, B), up_x), (at(0, every, x, B), dn_x),
+            ],
+            "s4": [
+                (at(0, yl, every, A), up_y), (at(1, yr, every, A), dn_y),
+                (at(0, every, xl, B), up_x), (at(1, every, xr, B), dn_x),
+            ],
+            "c1": [
+                (ct(zl, y, x, CA), up_x), (ct(zl, y, x, CA), dn_x),
+                (ct(zl, y, x, CB), up_y), (ct(zl, y, x, CB), dn_y),
+            ],
+            "c2": [
+                (ct(zl, y, xl, CA, t1), up_x), (ct(zl, y, xr, CA, t2), dn_x),
+                (ct(zl, yl, x, CB, t1), up_y), (ct(zl, yr, x, CB, t2), dn_y),
+            ],
+            "c3": [
+                (ct(zl, y, every, CA), up_y), (ct(zl, y, every, CA), dn_y),
+                (ct(zl, every, x, CB), up_x), (ct(zl, every, x, CB), dn_x),
+            ],
+            "c4": [
+                (ct(zl, yl, lo2, CA), up_y), (ct(zl, yr, hi2, CA), dn_y),
+                (ct(zl, lo2, xl, CB), up_x), (ct(zl, hi2, xr, CB), dn_x),
+            ],
+            "c5a": [
+                (ct(zl, lo2, every, mine_rows), z_next), (ct(zl, hi2, every, mine_rows), z_prev),
+            ],
+            "c5b": [
+                (ct(zl, hi2, every, mine_rows), z_next), (ct(zl, lo2, every, mine_rows), z_prev),
+            ],
+            "c6": [
+                (ct(away_zl, lo2, every, prev_rows), z_next),
+                (ct(away_zl, hi2, every, next_rows), z_prev),
+            ],
+        }
+
+    flights, landed = {}, set()
+
+    def land(k, s):
+        if (k, s) not in landed:
+            landed.add((k, s))
+            for c in flights[k, s]:
+                c.wait_recv()
+
+    def go(k, *names):
+        if k >= n:
             return
-        if s == 0:
-            own[k].wait()
+        steps = plan(k)
+        order = list(steps)
+        for s in names:
+            for before in needs[s]:
+                land(k, before)
+            base = sum(len(steps[o]) for o in order[: order.index(s)])
+            flights[k, s] = []
+            for i, (ref, target) in enumerate(steps[s]):
+                c = remote(ref, ref, target, send_sem.at[k, base + i], recv_sem.at[k, base + i])
+                c.start()
+                flights[k, s].append(c)
+
+    def done(k):
+        for s in needs:
+            land(k, s)
+
+    def stage_weights(k):
+        start = chunks[k][0]
+
+        def put(at, value):
+            W[zl, y, x, :, pl.ds(at, value.shape[1])] = value.astype(bf16)
+
+        if k < 2:
+            loads[k].wait()
+            put(start, (F1, F2)[k][...])
+        elif k == 2:
+            loads[2].wait()
+            put(start, F3[...].T)
         else:
-            land(k, s - 1)
-        base = sum(len(p) for p in plan(k)[:s])
-        flights[k, s] = []
-        for i, (ref, target) in enumerate(plan(k)[s]):
-            c = remote(ref, ref, target, send_sem.at[k, base + i], recv_sem.at[k, base + i])
-            c.start()
-            flights[k, s].append(c)
-
-    def land(k, s):
-        for c in flights[k, s]:
-            c.wait_recv()
-
+            if k == 3:
+                for c in loads[3:]:
+                    c.wait()
+            first, count = sum(GROUPS[: k - 3]), GROUPS[k - 3]
+            for t in range(count):
+                cut = slice((first + t) * LANES, (first + t + 1) * LANES)
+                put(start + t * 256, F4[:, cut])
+                put(start + t * 256 + LANES, F5[:, cut])
+            put(start + count * 256, F6[first * LANES : (first + count) * LANES, :].T)
+
+    stage_weights(0)
     pl.semaphore_wait(barrier, 7)
     swap_tok = remote(tok, X.at[tp], partner, tp_send.at[0], tp_recv.at[0])
     swap_tok.start()
-    for k in range(len(chunks)):
-        issue(k, 0)
-    issue(0, 1)
-    issue(1, 1)
+    go(0, "c1", "z0")
+    stage_weights(1)
+    stage_weights(2)
+    go(1, "c1", "z0")
+    go(0, "s1", "c2")
+    stage_weights(3)
+    go(2, "z0")
+    go(0, "s2", "c3")
+    stage_weights(4)
+    go(3, "z0")
+    stage_weights(5)
+    go(4, "z0")
+    go(0, "s3a", "s3b", "c4")
+    go(5, "z0")
+
+    def prepare():
+        zeros = jnp.zeros((64, 64), f32)
+        for g in range(half // LANES):
+            for p in range(2):
+                r = recur_ref[2 * g + p]
+                q = ingate_ref[2 * g + p]
+                parts = [r, zeros, q, zeros] if p == 0 else [zeros, r, zeros, q]
+                MAP[g, p * 64 : p * 64 + 64, :] = jnp.concatenate(parts, axis=1)
+        v = -decay_ref[...]
+        RATES[...] = -RATE * (jnp.maximum(v, 0.0) + jnp.log1p(jnp.exp(-jnp.abs(v))))
+        EX[...] = jnp.broadcast_to(extra_ref[...], (LANES, rows)).T
+
+    prepare()
     keep.wait()
     swap_tok.wait_recv()
 
@@ -161,11 +267,11 @@
             moved = jnp.where(row >= back, pltpu.roll(values, back, 0), 0.0)
             conv = conv + weights[taps - 1 - back : taps - back, :] * moved
         mapped = jnp.dot(
-            conv, map_ref[i], preferred_element_type=f32, precision=lax.Precision.HIGHEST
+            conv, MAP[i], preferred_element_type=f32, precision=lax.Precision.HIGHEST
         )
         recur = sigmoid(mapped[:, :LANES])
         ingate = sigmoid(mapped[:, LANES:])
-        log_rate = rate_ref[:, cols] * recur - extra_ref[...]
+        log_rate = RATES[:, cols] * recur - EX[...]
         a = jnp.exp(log_rate)
         u = -2.0 * log_rate
         series = u * (1 - u / 2 * (1 - u / 3 * (1 - u / 4 * (1 - u / 5 * (1 - u / 6)))))
@@ -217,26 +323,30 @@
         swap = remote(SB, RB, partner, tp_send.at[1], tp_recv.at[1])
         swap.start()
         lax.fori_loop(0, 4, mine_body, 0)
+        return swap
+
+    own_cols = pl.ds(pl.multiple_of(tp * half, half), half)
+
+    def mixer_mixed(swap):
         swap.wait_recv()
 
         def mixed_body(i, carry):
             r = pl.ds(pl.multiple_of(i * 64, 64), 64)
             total = PS[0, r, :] + RB[r, :].astype(f32)
-            X[tp, r, :] = (tok[r, :].astype(f32) + total * out_scale[...]).astype(bf16)
+            X[tp, r, :] = (tok[r, :].astype(f32) + total * out_scale[:, own_cols]).astype(bf16)
             return carry
 
         lax.fori_loop(0, rows // 64, mixed_body, 0)
         swap.wait_send()
         share = remote(X.at[tp], X.at[tp], partner, tp_send.at[2], tp_recv.at[2])
         share.start()
-        share.wait()
-        norm_rows(ffn_gain)
+        return share
 
     def hidden_tile(unit, start):
         cols = pl.ds(pl.multiple_of(unit * LANES, LANES), LANES)
         both = dot(N[...], wide(start, 256))
-        gate = both[:, :LANES] * fg_scale[:, cols]
-        lift = both[:, LANES:] * fu_scale[:, cols]
+        gate = both[:, :LANES] * fg_scale[cols].reshape(1, LANES)
+        lift = both[:, LANES:] * fu_scale[cols].reshape(1, LANES)
         H[:, cols] = (gate / (1.0 + jnp.exp(-gate)) * lift).astype(bf16)
 
     def ffn(g):
@@ -282,48 +392,72 @@
             def final(i, carry):
                 r = pl.ds(pl.multiple_of(i * 64, 64), 64)
                 total = PS[0, r, :] + RB2[r, :].astype(f32)
-                out_ref[r, :] = (X[tp, r, :].astype(f32) + total * dn_scale[...]).astype(bf16)
+                out_ref[r, :] = (X[tp, r, :].astype(f32) + total * dn_scale[:, own_cols]).astype(bf16)
                 return carry
 
             lax.fori_loop(0, rows // 64, final, 0)
 
-    issue(0, 2)
+    def slot_a(k):
+        go(k + 1, "c4")
+        go(k + 2, "c2")
+        go(k, "s3a", "s3b")
+        go(k + 1, "s2")
+        go(k + 2, "s1")
+        go(k, "c6")
+
+    def slot_b(k):
+        go(k + 2, "c3")
+        go(k + 3, "c1")
+        go(k, "s4")
+        go(k + 1, "c5a", "c5b")
+
+    def scans(first, last):
+        lax.fori_loop(first, last, scan_block, 0)
+
+    go(0, "c5a", "c5b")
+    go(1, "s1", "c2")
+    go(2, "c1", "s1")
     norm_rows(mix_gain)
-    issue(1, 2)
-    issue(0, 3)
-    issue(2, 1)
-    issue(0, 4)
-    issue(1, 3)
-    issue(2, 2)
-    issue(3, 1)
-    land(0, 4)
+    go(0, "s4")
+    go(1, "c3", "s2")
+    go(2, "c2")
+    go(0, "c6")
+    go(1, "c4")
+    go(2, "c3")
+    go(3, "c1")
+    go(1, "c5a", "c5b")
+    go(2, "c4")
+    go(3, "c2")
+    go(1, "s3a", "s3b")
+    go(2, "s2")
+    go(3, "s1")
+    done(0)
     branch_in()
-    lax.fori_loop(0, 2, scan_block, 0)
-    issue(1, 4)
-    issue(2, 3)
-    issue(3, 2)
-    issue(4, 1)
-    lax.fori_loop(2, 5, scan_block, 0)
-    land(1, 4)
-    issue(2, 4)
-    issue(3, 3)
-    issue(4, 2)
-    issue(5, 1)
-    lax.fori_loop(5, 8, scan_block, 0)
+    go(1, "c6")
+    slot_b(1)
+    scans(0, 3)
+    slot_a(2)
+    scans(3, 5)
+    slot_b(2)
+    scans(5, 8)
+    done(1)
     lax.fori_loop(0, 4, gate_block, 0)
-    issue(3, 4)
-    issue(4, 3)
-    issue(5, 2)
-    land(2, 4)
-    mixer_out()
-    issue(4, 4)
-    issue(5, 3)
-    land(3, 4)
+    slot_a(3)
+    done(2)
+    swap = mixer_out()
+    slot_b(3)
+    share = mixer_mixed(swap)
+    slot_a(4)
+    share.wait()
+    norm_rows(ffn_gain)
+    done(3)
     ffn(0)
-    issue(5, 4)
-    land(4, 4)
+    slot_b(4)
+    slot_a(5)
+    done(4)
     ffn(1)
-    land(5, 4)
+    slot_b(5)
+    done(5)
     ffn(2)
     swap_tok.wait_send()
     for group in flights.values():
@@ -337,46 +471,23 @@
         recur_gate, input_gate, decay_rate, extra_decay, lru_output, lru_output_scale, ffn_gain,
         ffn_gate, ffn_up, ffn_gate_scale, ffn_up_scale, ffn_down, ffn_down_scale,
     ) = args
-    tp = lax.axis_index("tp")
     rows, half = tokens.shape
     units = ffn_gate.shape[1] // LANES
-
-    out_t = lru_output.astype(bf16).T
-    down_t = ffn_down.astype(bf16).T
-    gate16, up16 = ffn_gate.astype(bf16), ffn_up.astype(bf16)
-    parts = [lru_input.astype(bf16), lru_gate.astype(bf16), out_t]
-    chunks = [(0, half), (half, half), (2 * half, half)]
+    chunks = [(k * half, half, 3 * LANES) for k in range(3)]
     first = 0
     for count in GROUPS:
-        for t in range(first, first + count):
-            cut = slice(t * LANES, (t + 1) * LANES)
-            parts += [gate16[:, cut], up16[:, cut]]
-        parts.append(down_t[:, first * LANES : (first + count) * LANES])
-        chunks.append((3 * half + first * 3 * LANES, count * 3 * LANES))
+        chunks.append((3 * half + first * 3 * LANES, count * 3 * LANES, (count + 1) * LANES))
         first += count
     assert first == units
-    piece = jnp.concatenate(parts, axis=1)
-    width = piece.shape[1]
-
-    per = LANES // recur_gate.shape[1]
-    groups = recur_gate.shape[0] // per
-
-    def block_diag(blocks):
-        tall = blocks.reshape(groups, LANES, blocks.shape[2])
-        both = jnp.concatenate([tall] * per, axis=2)
-        r = lax.broadcasted_iota(jnp.int32, both.shape, 1) // blocks.shape[1]
-        c = lax.broadcasted_iota(jnp.int32, both.shape, 2) // blocks.shape[2]
-        return jnp.where(r == c, both, 0.0)
-
-    maps = jnp.concatenate([block_diag(recur_gate), block_diag(input_gate)], axis=2)
-    rate = (-RATE * jax.nn.softplus(-decay_rate))[None, :]
-    mine = lambda v: lax.dynamic_slice_in_dim(v, tp * half, half)[None, :]
+    width = 3 * half + 3 * LANES * units
     n = len(chunks)
+    row = lambda v: v[None, :]
     vmem = pl.BlockSpec(memory_space=pltpu.VMEM)
+    hbm = pl.BlockSpec(memory_space=pl.ANY)
     return pl.pallas_call(
         functools.partial(layer_kernel, tuple(chunks)),
         out_shape=jax.ShapeDtypeStruct((rows, half), bf16),
-        in_specs=[vmem, pl.BlockSpec(memory_space=pl.ANY)] + [vmem] * 12,
+        in_specs=[vmem] + [hbm] * 6 + [vmem] * 13,
         out_specs=vmem,
         scratch_shapes=[
             pltpu.VMEM((2, 4, 4, 64, width), bf16),
@@ -390,20 +501,30 @@
             pltpu.VMEM((rows, half), bf16),
             pltpu.VMEM((rows, units * LANES), bf16),
             pltpu.VMEM((2, rows, half), f32),
-            pltpu.SemaphoreType.DMA((n, 18)),
-            pltpu.SemaphoreType.DMA((n, 18)),
+            pltpu.VMEM(lru_input.shape, f32),
+            pltpu.VMEM(lru_gate.shape, f32),
+            pltpu.VMEM(lru_output.shape, f32),
+            pltpu.VMEM(ffn_gate.shape, f32),
+            pltpu.VMEM(ffn_up.shape, f32),
+            pltpu.VMEM(ffn_down.shape, f32),
+            pltpu.VMEM((half // LANES, LANES, 2 * LANES), f32),
+            pltpu.VMEM((1, half), f32),
+            pltpu.VMEM((rows, LANES), f32),
+            pltpu.SemaphoreType.DMA((n, 44)),
+            pltpu.SemaphoreType.DMA((n, 44)),
             pltpu.SemaphoreType.DMA((4,)),
             pltpu.SemaphoreType.DMA((4,)),
-            pltpu.SemaphoreType.DMA((n + 1,)),
+            pltpu.SemaphoreType.DMA((7,)),
         ],
         compiler_params=pltpu.CompilerParams(
             collective_id=0, has_side_effects=True, vmem_limit_bytes=67043328
         ),
         name="layer",
     )(
-        tokens, piece, mix_gain[None, :], lru_input_scale[None, :], lru_gate_scale[None, :],
-        conv_weight, maps, rate, extra_decay[:, None], mine(lru_output_scale), ffn_gain[None, :],
-        ffn_gate_scale[None, :], ffn_up_scale[None, :], mine(ffn_down_scale),
+        tokens, lru_input, lru_gate, lru_output, ffn_gate, ffn_up, ffn_down, row(mix_gain),
+        row(lru_input_scale), row(lru_gate_scale), conv_weight, recur_gate, input_gate,
+        row(decay_rate), row(extra_decay), row(lru_output_scale), row(ffn_gain),
+        ffn_gate_scale, ffn_up_scale, row(ffn_down_scale),
     )
 
 

time: 209 us -> 147 us (0.70)
  Pallas kernels: 177 us -> 142 us
  local copies, waits for them, and re-layouts: 25.8 us -> 5.42 us
  other arithmetic: 5.87 us -> 0 us
    pallas_call x1, Pallas kernels: 177 us -> 142 us  [local(): pl.pallas_call(functools.partial(layer_kernel, tuple(chunks)), out_shape=...]
    unnamed x41 -> x5, local copies, waits for them, and re-layouts: 19.1 us -> 5.42 us
    broadcast_in_dim x3 -> x0, local copies, waits for them, and re-layouts: 3.45 us -> none  [the longest x1 1.29 us: local(): ffn_up_scale[None, :]]
    dynamic_slice x2 -> x0, local copies, waits for them, and re-layouts: 2.55 us -> none  [local(): mine = lambda v: lax.dynamic_slice_in_dim(v, tp * half, half)[None, :]]
where the time goes in v1:
time: 147 us
  Pallas kernels  142 us (97%)
  local copies, waits for them, and re-layouts  5.42 us (4%)
    pallas_call x1, Pallas kernels, local(): pl.pallas_call(functools.partial(layer_kernel, tuple(chunks)), out_shape=...  142 us
    unnamed x5, local copies, waits for them, and re-layouts  5.42 us

profile of v1, /device:TPU:1, one launch (start us, length us, event | category | flops | bytes accessed | tf_op | source)
XLA Modules:
  0.0 147.1 jit_solution(10030388520756493607)
XLA Ops:
  0.0 0.0 copy-start
  0.0 2.0 %copy.21.w_out = f32[1024,64]{1,0:T(8,128)} copy(f32[1024,64]{0,1:T(8,128)} %param.31) | data formatting | bytes 524288 | tf_op args[11]
  2.0 0.0 copy-done
  2.0 1.1 copy.22.w_dn
  3.2 141.7 %layer.1 = bf16[512,1024]{1,0:T(8,128)(2,1)} custom-call(bf16[512,1024]{1,0:T(8,128)(2,1)} %tok.1, f32[64,1024]{1,0:T(8,128)} %w_in.1, f32[64,1024]{1,0:T(8,128)} %w_gate.1, f32[1024,64]{1,0:T(8,128)} %copy.21.w_out, f32[64,1408]{1,0:T(8,128)} %w_fg.1, f32[64,1408]{1,0:T(8,128)} %w_fu.1, f32[1408,64]{1,0:T(8,128)} %copy.22.w_dn, f32[1,2048]{1,0:T(1,128)} %bitcast.8, ...), custom_call_target="tpu_custom_call" | custom-call | tf_op jit(solution)/shard_map/layer/pallas_call | solution.py:487
  144.8 2.3 %copy.24 = bf16[512,1024]{1,0:T(8,128)(2,1)} copy(bf16[512,1024]{1,0:T(8,128)(2,1)} %layer.1) | data formatting | bytes 2097152
Async XLA Ops:
  0.0 2.0 %copy-start = (f32[1408,64]{0,1:T(8,128)S(1)}, f32[1408,64]{0,1:T(8,128)}, u32[]{:S(2)}) copy-start(f32[1408,64]{0,1:T(8,128)} %param.38) | copy-start | bytes 1081348

commit v2 on v1

--- a/solution.py
+++ b/solution.py
@@ -11,8 +11,95 @@
 RATE = 8.0
 LANES = 128
 MESH = pl.DeviceIdType.MESH
-GROUPS = (4, 4, 3)
+NEEDS = {
+    "z0": (), "s1": ("z0",), "s2": ("s1",), "s3a": ("s2",), "s3b": ("s2",), "s4": ("s3a",),
+    "c1": (), "c2": ("c1",), "c3": ("c2",), "c4": ("c3",), "c5a": ("c4",), "c5b": ("c4",),
+    "c6": ("c5a",),
+}
+TILES = (8, 8, 8, 8, 8, 6, 8, 3)
+LAST = (2, 0, 5, 5, 5, 2, 2, 0)
+PRIORITY = (-3.8, 0.7, -15.5, -6.8, 3.8, -2.3, -0.6, -9.8, -0.1, -8.1, 10.2, 13.8, -22.0)
+BACKLOG = 3.5
 f32, bf16 = jnp.float32, jnp.bfloat16
+
+
+def stage_bytes(width, last):
+    first, cut = width - last, (last // LANES + 1) // 2 * LANES
+    plane = lambda r, w: {d: r * w for d in range(4)}
+    depth = lambda r, w: {d: r * w for d in (4, 5)}
+    sizes = {
+        "z0": depth(32, first), "s1": plane(64, first), "s2": plane(32, first),
+        "s3a": plane(128, first), "s3b": plane(128, first), "s4": plane(128, first),
+        "c1": plane(16, last), "c2": plane(16, cut), "c3": plane(64, last), "c4": plane(32, last),
+        "c5a": depth(256, last), "c5b": depth(256, last), "c6": depth(256, last),
+    }
+    return {s: v for s, v in sizes.items() if sum(v.values()) > 0}
+
+
+def arrange(chunks, work, latency=2.4, rate=46650.0):
+    count, steps = len(chunks), list(NEEDS)
+    sizes = [stage_bytes(width, last) for _, width, last in chunks]
+    free, land, staged, ended = [0.0] * 6, {}, [None] * count, {}
+    todo = [(k, s) for k in range(count) for s in sizes[k]]
+    todo.sort(key=lambda c: (c[0] + PRIORITY[steps.index(c[1])], steps.index(c[1])))
+    order, now, work, never = [], 0.0, list(work), 1e9
+    whole = lambda k: max(land.get((k, s), never) for s in sizes[k])
+    while todo or work:
+        pick, later = None, never
+        for k, s in todo:
+            if staged[k] is None:
+                continue
+            ready = max(
+                [staged[k]] + [land.get((k, d), never) for d in NEEDS[s] if d in sizes[k]]
+            )
+            queue = max(free[d] for d in sizes[k][s]) - now
+            if ready > now:
+                later = min(later, ready)
+            elif queue > BACKLOG:
+                later = min(later, now + queue - BACKLOG + 1e-6)
+            else:
+                pick = (k, s)
+                break
+        if pick:
+            k, s = pick
+            todo.remove(pick)
+            order.append(pick)
+            for d, size in sizes[k][s].items():
+                free[d] = max(free[d], now) + size * 2 / rate
+            land[pick] = max(free[d] for d in sizes[k][s]) + latency
+            now += 0.15
+            continue
+        if work:
+            name, cost, reads, after = work[0]
+            ready = max(
+                [0.0] + [whole(k) for k in reads] + [ended[w] + delay for w, delay in after]
+            )
+            if ready <= now:
+                work.pop(0)
+                order.append((-1, name))
+                now += cost
+                ended[name] = now
+                if name[:5] == "stage":
+                    staged[int(name[5:])] = now
+                continue
+            if ready < never:
+                later = min(later, ready)
+        now = later
+    return order
+
+
+WORK = (
+    tuple((f"stage{k}", 0.4, (), ()) for k in range(len(TILES)))
+    + (("prep", 1.0, (), ()), ("norm1", 1.5, (), ()), ("in", 3.8, (0,), ()))
+    + tuple((f"scan{i}", 3.3, (), ()) for i in range(4))
+    + (
+        ("gate0", 2.4, (1,), ()), ("gate1", 2.4, (), ()), ("outA", 2.2, (2,), ()),
+        ("outH", 2.2, (), ()), ("mixed", 1.0, (), (("outA", 3.0),)),
+        ("norm2", 1.5, (), (("mixed", 3.2),)), ("hid0", 4.0, (3,), ()), ("hid1", 4.0, (4,), ()),
+        ("hid2", 3.0, (5,), ()), ("downA", 2.5, (6,), ()), ("downH", 2.5, (), ()),
+        ("last", 4.0, (7,), ()),
+    )
+)
 
 
 def sigmoid(v):
@@ -23,12 +110,12 @@
     chunks, tok, w_in, w_gate, w_out, w_fg, w_fu, w_dn,
     mix_gain, in_scale, gt_scale, conv_ref, recur_ref, ingate_ref, decay_ref, extra_ref,
     out_scale, ffn_gain, fg_scale, fu_scale, dn_scale, out_ref,
-    W, X, N, BI, ST, GA, SB, RB, RB2, H, PS, F1, F2, F3, F4, F5, F6, MAP, RATES, EX,
+    W, X, N, BI, ST, GA, SB, RB, RB2, H, PS, F1, F2, F3, F4, F5, F6, F7, F8, MAP, RATES, EX,
     send_sem, recv_sem, tp_send, tp_recv, own_sem,
 ):
     rep, fs, tp = lax.axis_index("rep"), lax.axis_index("fs"), lax.axis_index("tp")
     zl, y, x = fs // 16, (fs // 4) % 4, fs % 4
-    rows, half = tok.shape
+    rows, half = X.shape[1:]
     n = len(chunks)
     up = lambda v: lax.rem(v + 1, 4)
     dn = lambda v: lax.rem(v + 3, 4)
@@ -48,13 +135,15 @@
 
     loads = []
     for i, (src, dst) in enumerate(
-        [(w_in, F1), (w_gate, F2), (w_out, F3), (w_fg, F4), (w_fu, F5), (w_dn, F6)]
+        [
+            (w_in, F1), (tok, X.at[tp]), (w_gate, F2), (w_out, F3), (w_fg, F4), (w_fu, F5),
+            (w_dn, F6), (recur_ref, F7), (ingate_ref, F8),
+        ]
     ):
         c = pltpu.make_async_copy(src, dst, own_sem.at[i])
         c.start()
         loads.append(c)
-    keep = pltpu.make_async_copy(tok, X.at[tp], own_sem.at[6])
-    keep.start()
+    keep = loads.pop(1)
 
     def remote(src, dst, target, ssem, rsem):
         return pltpu.make_async_remote_copy(
@@ -71,12 +160,6 @@
     next_rows = pl.ds(pl.multiple_of(rep_next * 32, 32), 32)
     prev_rows = pl.ds(pl.multiple_of(rep_prev * 32, 32), 32)
     up_x, dn_x, up_y, dn_y = to_x(xr), to_x(xl), to_y(yr), to_y(yl)
-    needs = {
-        "z0": (), "s1": ("z0",), "s2": ("s1",), "s3a": ("s2",), "s3b": ("s2",), "s4": ("s3a",),
-        "c1": (), "c2": ("c1",), "c3": ("c2",), "c4": ("c3",), "c5a": ("c4",), "c5b": ("c4",),
-        "c6": ("c5a",),
-    }
-
     def plan(k):
         start, width, last = chunks[k]
         cols, tail = pl.ds(start, width - last), pl.ds(start + width - last, last)
@@ -84,8 +167,8 @@
         t1 = pl.ds(start + width - last, cut)
         t2 = pl.ds(start + width - last + cut, last - cut)
         at = lambda a, b, c, r: W.at[a, b, c, r, cols]
-        ct = lambda a, b, c, r, t=tail: W.at[a, b, c, r, t]
-        return {
+        ct = lambda a, b, c, r, t=tail: W.at[a, b, c, r, t] if t.size else None
+        steps = {
             "z0": [(at(zl, y, x, A), z_next), (at(zl, y, x, B), z_prev)],
             "s1": [
                 (at(every, y, x, A), up_x), (at(every, y, x, A), dn_x),
@@ -134,6 +217,9 @@
                 (ct(away_zl, hi2, every, next_rows), z_prev),
             ],
         }
+        steps["c2"] = steps["c2"] if last > cut else steps["c2"][::2]
+        sizes = stage_bytes(width, last)
+        return {s: v for s, v in steps.items() if s in sizes}
 
     flights, landed = {}, set()
 
@@ -143,23 +229,21 @@
             for c in flights[k, s]:
                 c.wait_recv()
 
-    def go(k, *names):
-        if k >= n:
-            return
+    def go(k, s):
         steps = plan(k)
         order = list(steps)
-        for s in names:
-            for before in needs[s]:
+        for before in NEEDS[s]:
+            if before in steps:
                 land(k, before)
-            base = sum(len(steps[o]) for o in order[: order.index(s)])
-            flights[k, s] = []
-            for i, (ref, target) in enumerate(steps[s]):
-                c = remote(ref, ref, target, send_sem.at[k, base + i], recv_sem.at[k, base + i])
-                c.start()
-                flights[k, s].append(c)
+        base = sum(len(steps[o]) for o in order[: order.index(s)])
+        flights[k, s] = []
+        for i, (ref, target) in enumerate(steps[s]):
+            c = remote(ref, ref, target, send_sem.at[k, base + i], recv_sem.at[k, base + i])
+            c.start()
+            flights[k, s].append(c)
 
     def done(k):
-        for s in needs:
+        for s in plan(k):
             land(k, s)
 
     def stage_weights(k):
@@ -168,57 +252,40 @@
         def put(at, value):
             W[zl, y, x, :, pl.ds(at, value.shape[1])] = value.astype(bf16)
 
-        if k < 2:
+        if k < 3:
             loads[k].wait()
-            put(start, (F1, F2)[k][...])
-        elif k == 2:
-            loads[2].wait()
-            put(start, F3[...].T)
-        else:
+            put(start, (F1, F2, F3)[k][...])
+        elif k < 6:
             if k == 3:
-                for c in loads[3:]:
-                    c.wait()
-            first, count = sum(GROUPS[: k - 3]), GROUPS[k - 3]
-            for t in range(count):
-                cut = slice((first + t) * LANES, (first + t + 1) * LANES)
+                loads[3].wait()
+                loads[4].wait()
+            for t, unit in enumerate(units_of(k)):
+                cut = slice(unit * LANES, (unit + 1) * LANES)
                 put(start + t * 256, F4[:, cut])
                 put(start + t * 256 + LANES, F5[:, cut])
-            put(start + count * 256, F6[first * LANES : (first + count) * LANES, :].T)
-
-    stage_weights(0)
-    pl.semaphore_wait(barrier, 7)
-    swap_tok = remote(tok, X.at[tp], partner, tp_send.at[0], tp_recv.at[0])
-    swap_tok.start()
-    go(0, "c1", "z0")
-    stage_weights(1)
-    stage_weights(2)
-    go(1, "c1", "z0")
-    go(0, "s1", "c2")
-    stage_weights(3)
-    go(2, "z0")
-    go(0, "s2", "c3")
-    stage_weights(4)
-    go(3, "z0")
-    stage_weights(5)
-    go(4, "z0")
-    go(0, "s3a", "s3b", "c4")
-    go(5, "z0")
+        else:
+            if k == 6:
+                loads[5].wait()
+            first = start - chunks[6][0]
+            put(start, F6[:, first : first + chunks[k][1]])
+
+    def units_of(k):
+        first = (chunks[k][0] - chunks[3][0]) // 256
+        return range(first, first + chunks[k][1] // 256)
 
     def prepare():
         zeros = jnp.zeros((64, 64), f32)
+        loads[6].wait()
+        loads[7].wait()
         for g in range(half // LANES):
             for p in range(2):
-                r = recur_ref[2 * g + p]
-                q = ingate_ref[2 * g + p]
+                r = F7[2 * g + p]
+                q = F8[2 * g + p]
                 parts = [r, zeros, q, zeros] if p == 0 else [zeros, r, zeros, q]
                 MAP[g, p * 64 : p * 64 + 64, :] = jnp.concatenate(parts, axis=1)
         v = -decay_ref[...]
         RATES[...] = -RATE * (jnp.maximum(v, 0.0) + jnp.log1p(jnp.exp(-jnp.abs(v))))
         EX[...] = jnp.broadcast_to(extra_ref[...], (LANES, rows)).T
-
-    prepare()
-    keep.wait()
-    swap_tok.wait_recv()
 
     def norm_rows(gain):
         step = 64
@@ -308,39 +375,32 @@
     def rows_of(block, j, start, width):
         return W[block, j, :, :, pl.ds(start, width)].reshape(256, width)
 
-    def mixer_out():
-        def send_body(j, carry):
+    own_cols = pl.ds(pl.multiple_of(tp * half, half), half)
+
+    def out_away():
+        def body(j, carry):
             cols = pl.ds(pl.multiple_of(j * 256, 256), 256)
             SB[:, cols] = dot_t(GA[...], rows_of(other, j, 2 * half, half)).astype(bf16)
             return carry
 
-        def mine_body(j, carry):
+        lax.fori_loop(0, 4, body, 0)
+
+    def out_home():
+        def body(j, carry):
             cols = pl.ds(pl.multiple_of(j * 256, 256), 256)
             PS[0, :, cols] = dot_t(GA[...], rows_of(tp, j, 2 * half, half))
             return carry
 
-        lax.fori_loop(0, 4, send_body, 0)
-        swap = remote(SB, RB, partner, tp_send.at[1], tp_recv.at[1])
-        swap.start()
-        lax.fori_loop(0, 4, mine_body, 0)
-        return swap
-
-    own_cols = pl.ds(pl.multiple_of(tp * half, half), half)
-
-    def mixer_mixed(swap):
-        swap.wait_recv()
-
-        def mixed_body(i, carry):
+        lax.fori_loop(0, 4, body, 0)
+
+    def mix_rows():
+        def body(i, carry):
             r = pl.ds(pl.multiple_of(i * 64, 64), 64)
             total = PS[0, r, :] + RB[r, :].astype(f32)
-            X[tp, r, :] = (tok[r, :].astype(f32) + total * out_scale[:, own_cols]).astype(bf16)
-            return carry
-
-        lax.fori_loop(0, rows // 64, mixed_body, 0)
-        swap.wait_send()
-        share = remote(X.at[tp], X.at[tp], partner, tp_send.at[2], tp_recv.at[2])
-        share.start()
-        return share
+            X[tp, r, :] = (X[tp, r, :].astype(f32) + total * out_scale[:, own_cols]).astype(bf16)
+            return carry
+
+        lax.fori_loop(0, rows // 64, body, 0)
 
     def hidden_tile(unit, start):
         cols = pl.ds(pl.multiple_of(unit * LANES, LANES), LANES)
@@ -349,117 +409,114 @@
         lift = both[:, LANES:] * fu_scale[cols].reshape(1, LANES)
         H[:, cols] = (gate / (1.0 + jnp.exp(-gate)) * lift).astype(bf16)
 
-    def ffn(g):
-        first, count = sum(GROUPS[:g]), GROUPS[g]
-        start = 3 * half + first * 3 * LANES
+    def hidden(k):
+        units, start = units_of(k), chunks[k][0]
         lax.fori_loop(
-            0, count,
-            lambda t, c: (hidden_tile(first + t, pl.multiple_of(start + t * 256, 128)), c)[1], 0,
+            0, len(units),
+            lambda t, c: (
+                hidden_tile(units[0] + t, pl.multiple_of(start + t * 256, 128)), c
+            )[1], 0,
         )
-        down = start + count * 256
-        acts = lambda: H[:, first * LANES : (first + count) * LANES]
-
-        def part(slot, block, j):
+
+    def down(k, block, j):
+        start, width, _ = chunks[k]
+        first = start - chunks[6][0]
+        return dot_t(H[:, first : first + width], rows_of(block, j, start, width))
+
+    def down_body(k, slot, block):
+        def body(j, carry):
             cols = pl.ds(pl.multiple_of(j * 256, 256), 256)
-            v = dot_t(acts(), rows_of(block, j, down, count * LANES))
-            if g > 0:
-                v = PS[slot, :, cols] + v
-            return cols, v
-
-        last = g == len(GROUPS) - 1
-
+            PS[slot, :, cols] = down(k, block, j)
+            return carry
+
+        lax.fori_loop(0, 4, body, 0)
+
+    def finish(k):
         def away(j, carry):
-            cols, v = part(1, other, j)
-            if last:
-                SB[:, cols] = v.astype(bf16)
-            else:
-                PS[1, :, cols] = v
+            cols = pl.ds(pl.multiple_of(j * 256, 256), 256)
+            SB[:, cols] = (PS[1, :, cols] + down(k, other, j)).astype(bf16)
             return carry
 
         def home(j, carry):
-            cols, v = part(0, tp, j)
-            PS[0, :, cols] = v
-            return carry
-
-        lax.fori_loop(0, 4, away, 0)
-        if last:
-            swap = remote(SB, RB2, partner, tp_send.at[3], tp_recv.at[3])
-            swap.start()
-        lax.fori_loop(0, 4, home, 0)
-        if last:
-            swap.wait()
-
-            def final(i, carry):
-                r = pl.ds(pl.multiple_of(i * 64, 64), 64)
-                total = PS[0, r, :] + RB2[r, :].astype(f32)
-                out_ref[r, :] = (X[tp, r, :].astype(f32) + total * dn_scale[:, own_cols]).astype(bf16)
-                return carry
-
-            lax.fori_loop(0, rows // 64, final, 0)
-
-    def slot_a(k):
-        go(k + 1, "c4")
-        go(k + 2, "c2")
-        go(k, "s3a", "s3b")
-        go(k + 1, "s2")
-        go(k + 2, "s1")
-        go(k, "c6")
-
-    def slot_b(k):
-        go(k + 2, "c3")
-        go(k + 3, "c1")
-        go(k, "s4")
-        go(k + 1, "c5a", "c5b")
-
-    def scans(first, last):
-        lax.fori_loop(first, last, scan_block, 0)
-
-    go(0, "c5a", "c5b")
-    go(1, "s1", "c2")
-    go(2, "c1", "s1")
-    norm_rows(mix_gain)
-    go(0, "s4")
-    go(1, "c3", "s2")
-    go(2, "c2")
-    go(0, "c6")
-    go(1, "c4")
-    go(2, "c3")
-    go(3, "c1")
-    go(1, "c5a", "c5b")
-    go(2, "c4")
-    go(3, "c2")
-    go(1, "s3a", "s3b")
-    go(2, "s2")
-    go(3, "s1")
-    done(0)
-    branch_in()
-    go(1, "c6")
-    slot_b(1)
-    scans(0, 3)
-    slot_a(2)
-    scans(3, 5)
-    slot_b(2)
-    scans(5, 8)
-    done(1)
-    lax.fori_loop(0, 4, gate_block, 0)
-    slot_a(3)
-    done(2)
-    swap = mixer_out()
-    slot_b(3)
-    share = mixer_mixed(swap)
-    slot_a(4)
-    share.wait()
-    norm_rows(ffn_gain)
-    done(3)
-    ffn(0)
-    slot_b(4)
-    slot_a(5)
-    done(4)
-    ffn(1)
-    slot_b(5)
-    done(5)
-    ffn(2)
-    swap_tok.wait_send()
+            c = pl.multiple_of(j * 256, 256)
+            cols = pl.ds(c, 256)
+            scale = dn_scale[:, pl.ds(pl.multiple_of(tp * half + c, 256), 256)]
+            total = PS[0, :, cols] + down(k, tp, j) + RB2[:, cols].astype(f32)
+            out_ref[:, cols] = (X[tp, :, cols].astype(f32) + total * scale).astype(bf16)
+            return carry
+
+        swaps = []
+        for i in range(2):
+            lax.fori_loop(2 * i, 2 * i + 2, away, 0)
+            cols = pl.ds(i * (half // 2), half // 2)
+            c = remote(SB.at[:, cols], RB2.at[:, cols], partner, tp_send.at[3 + i], tp_recv.at[3 + i])
+            c.start()
+            swaps.append(c)
+        for i in range(2):
+            swaps[i].wait_recv()
+            lax.fori_loop(2 * i, 2 * i + 2, home, 0)
+        for c in swaps:
+            c.wait_send()
+
+    swap_tok = remote(X.at[tp], X.at[tp], partner, tp_send.at[0], tp_recv.at[0])
+    swap_out = remote(SB, RB, partner, tp_send.at[1], tp_recv.at[1])
+    swap_mix = remote(X.at[tp], X.at[tp], partner, tp_send.at[2], tp_recv.at[2])
+
+    def compute(name):
+        if name == "stage0":
+            stage_weights(0)
+            pl.semaphore_wait(barrier, 7)
+        elif name[:5] == "stage":
+            stage_weights(int(name[5:]))
+            if name == "stage1":
+                keep.wait()
+                swap_tok.start()
+        elif name == "prep":
+            prepare()
+        elif name == "norm1":
+            swap_tok.wait()
+            norm_rows(mix_gain)
+        elif name == "in":
+            done(0)
+            branch_in()
+        elif name[:4] == "scan":
+            i = int(name[4:])
+            lax.fori_loop(2 * i, 2 * i + 2, scan_block, 0)
+        elif name[:4] == "gate":
+            done(1)
+            i = int(name[4:])
+            lax.fori_loop(2 * i, 2 * i + 2, gate_block, 0)
+        elif name == "outA":
+            done(2)
+            out_away()
+            swap_out.start()
+        elif name == "outH":
+            out_home()
+        elif name == "mixed":
+            swap_out.wait()
+            mix_rows()
+            swap_mix.start()
+        elif name == "norm2":
+            swap_mix.wait()
+            norm_rows(ffn_gain)
+        elif name[:3] == "hid":
+            k = 3 + int(name[3:])
+            done(k)
+            hidden(k)
+        elif name == "downA":
+            done(6)
+            down_body(6, 1, other)
+        elif name == "downH":
+            down_body(6, 0, tp)
+        else:
+            done(7)
+            finish(7)
+
+    for k, name in arrange(chunks, WORK):
+        if k < 0:
+            compute(name)
+        else:
+            go(k, name)
     for group in flights.values():
         for c in group:
             c.wait_send()
@@ -473,13 +530,12 @@
     ) = args
     rows, half = tokens.shape
     units = ffn_gate.shape[1] // LANES
-    chunks = [(k * half, half, 3 * LANES) for k in range(3)]
-    first = 0
-    for count in GROUPS:
-        chunks.append((3 * half + first * 3 * LANES, count * 3 * LANES, (count + 1) * LANES))
-        first += count
-    assert first == units
-    width = 3 * half + 3 * LANES * units
+    chunks, width = [], 0
+    for tiles, last in zip(TILES, LAST):
+        chunks.append((width, tiles * LANES, last * LANES))
+        width += tiles * LANES
+    assert sum(TILES[:3]) * LANES == 3 * half and sum(TILES[3:6]) == 2 * units
+    assert sum(TILES[6:]) == units
     n = len(chunks)
     row = lambda v: v[None, :]
     vmem = pl.BlockSpec(memory_space=pltpu.VMEM)
@@ -487,7 +543,7 @@
     return pl.pallas_call(
         functools.partial(layer_kernel, tuple(chunks)),
         out_shape=jax.ShapeDtypeStruct((rows, half), bf16),
-        in_specs=[vmem] + [hbm] * 6 + [vmem] * 13,
+        in_specs=[hbm] * 7 + [vmem] * 4 + [hbm] * 2 + [vmem] * 7,
         out_specs=vmem,
         scratch_shapes=[
             pltpu.VMEM((2, 4, 4, 64, width), bf16),
@@ -503,25 +559,27 @@
             pltpu.VMEM((2, rows, half), f32),
             pltpu.VMEM(lru_input.shape, f32),
             pltpu.VMEM(lru_gate.shape, f32),
-            pltpu.VMEM(lru_output.shape, f32),
+            pltpu.VMEM(lru_output.shape[::-1], f32),
             pltpu.VMEM(ffn_gate.shape, f32),
             pltpu.VMEM(ffn_up.shape, f32),
-            pltpu.VMEM(ffn_down.shape, f32),
+            pltpu.VMEM(ffn_down.shape[::-1], f32),
+            pltpu.VMEM(recur_gate.shape, f32),
+            pltpu.VMEM(input_gate.shape, f32),
             pltpu.VMEM((half // LANES, LANES, 2 * LANES), f32),
             pltpu.VMEM((1, half), f32),
             pltpu.VMEM((rows, LANES), f32),
             pltpu.SemaphoreType.DMA((n, 44)),
             pltpu.SemaphoreType.DMA((n, 44)),
-            pltpu.SemaphoreType.DMA((4,)),
-            pltpu.SemaphoreType.DMA((4,)),
-            pltpu.SemaphoreType.DMA((7,)),
+            pltpu.SemaphoreType.DMA((5,)),
+            pltpu.SemaphoreType.DMA((5,)),
+            pltpu.SemaphoreType.DMA((9,)),
         ],
         compiler_params=pltpu.CompilerParams(
             collective_id=0, has_side_effects=True, vmem_limit_bytes=67043328
         ),
         name="layer",
     )(
-        tokens, lru_input, lru_gate, lru_output, ffn_gate, ffn_up, ffn_down, row(mix_gain),
+        tokens, lru_input, lru_gate, lru_output.T, ffn_gate, ffn_up, ffn_down.T, row(mix_gain),
         row(lru_input_scale), row(lru_gate_scale), conv_weight, recur_gate, input_gate,
         row(decay_rate), row(extra_decay), row(lru_output_scale), row(ffn_gain),
         ffn_gate_scale, ffn_up_scale, row(ffn_down_scale),

time: 147 us -> 137 us (0.932)
  Pallas kernels: 142 us -> 134 us
  local copies, waits for them, and re-layouts: 5.42 us -> 2.26 us
    pallas_call x1, Pallas kernels: 142 us -> 134 us  [local(): pl.pallas_call(functools.partial(layer_kernel, tuple(chunks)), out_shape=...]
    unnamed x5 -> x1, local copies, waits for them, and re-layouts: 5.42 us -> 2.26 us
where the time goes in v2:
time: 137 us
  Pallas kernels  134 us (98%)
  local copies, waits for them, and re-layouts  2.26 us (2%)
    pallas_call x1, Pallas kernels, local(): pl.pallas_call(functools.partial(layer_kernel, tuple(chunks)), out_shape=...  134 us

profile of v2, /device:TPU:1, one launch (start us, length us, event | category | flops | bytes accessed | tf_op | source)
XLA Modules:
  0.0 136.6 jit_solution(7762614547856585260)
XLA Ops:
  0.0 134.4 %layer.1 = bf16[512,1024]{1,0:T(8,128)(2,1)} custom-call(bf16[512,1024]{1,0:T(8,128)(2,1)} %tok.1, f32[64,1024]{1,0:T(8,128)} %w_in.1, f32[64,1024]{1,0:T(8,128)} %w_gate.1, f32[64,1024]{1,0:T(8,128)} %bitcast.11, f32[64,1408]{1,0:T(8,128)} %w_fg.1, f32[64,1408]{1,0:T(8,128)} %w_fu.1, f32[64,1408]{1,0:T(8,128)} %bitcast.10, f32[1,2048]{1,0:T(1,128)} %bitcast.12, ...), custom_call_target="tpu_custom_call" | custom-call | tf_op jit(solution)/shard_map/layer/pallas_call | solution.py:543
  134.4 2.3 %copy.22 = bf16[512,1024]{1,0:T(8,128)(2,1)} copy(bf16[512,1024]{1,0:T(8,128)(2,1)} %layer.1) | data formatting | bytes 2097152

commit v3 on v2

--- a/solution.py
+++ b/solution.py
@@ -17,9 +17,10 @@
     "c6": ("c5a",),
 }
 TILES = (8, 8, 8, 8, 8, 6, 8, 3)
-LAST = (2, 0, 5, 5, 5, 2, 2, 0)
-PRIORITY = (-3.8, 0.7, -15.5, -6.8, 3.8, -2.3, -0.6, -9.8, -0.1, -8.1, 10.2, 13.8, -22.0)
-BACKLOG = 3.5
+LAST = (3, 4, 7, 0, 4, 2, 1, 1)
+PRIORITY = (12.9, 0.9, 3.5, -7.5, 10.2, 10.3, -10.0, 3.7, -5.9, 2.9, 3.5, 7.4, 7.5)
+VMEM = 67043328
+BACKLOG = 2.0
 f32, bf16 = jnp.float32, jnp.bfloat16
 
 
@@ -36,7 +37,7 @@
     return {s: v for s, v in sizes.items() if sum(v.values()) > 0}
 
 
-def arrange(chunks, work, latency=2.4, rate=46650.0):
+def arrange(chunks, work, latency=2.2, rate=46650.0):
     count, steps = len(chunks), list(NEEDS)
     sizes = [stage_bytes(width, last) for _, width, last in chunks]
     free, land, staged, ended = [0.0] * 6, {}, [None] * count, {}
@@ -89,15 +90,15 @@
 
 
 WORK = (
-    tuple((f"stage{k}", 0.4, (), ()) for k in range(len(TILES)))
-    + (("prep", 1.0, (), ()), ("norm1", 1.5, (), ()), ("in", 3.8, (0,), ()))
-    + tuple((f"scan{i}", 3.3, (), ()) for i in range(4))
+    tuple((f"stage{k}", 0.35, (), ()) for k in range(len(TILES)))
+    + (("prep", 1.0, (), ()), ("norm1", 1.1, (), ()), ("in", 2.8, (0,), ()))
+    + tuple((f"scan{i}", 2.4, (), ()) for i in range(4))
     + (
-        ("gate0", 2.4, (1,), ()), ("gate1", 2.4, (), ()), ("outA", 2.2, (2,), ()),
-        ("outH", 2.2, (), ()), ("mixed", 1.0, (), (("outA", 3.0),)),
-        ("norm2", 1.5, (), (("mixed", 3.2),)), ("hid0", 4.0, (3,), ()), ("hid1", 4.0, (4,), ()),
-        ("hid2", 3.0, (5,), ()), ("downA", 2.5, (6,), ()), ("downH", 2.5, (), ()),
-        ("last", 4.0, (7,), ()),
+        ("gate0", 1.7, (1,), ()), ("gate1", 1.7, (), ()), ("outA", 1.6, (2,), ()),
+        ("outH", 1.6, (), ()), ("mixed", 0.8, (), (("outA", 3.0),)),
+        ("norm2", 1.1, (), (("mixed", 3.2),)), ("hid0", 2.9, (3,), ()), ("hid1", 2.9, (4,), ()),
+        ("hid2", 2.2, (5,), ()), ("downA", 1.8, (6,), ()), ("downH", 1.8, (), ()),
+        ("last", 3.0, (7,), ()),
     )
 )
 
@@ -108,11 +109,18 @@
 
 def layer_kernel(
     chunks, tok, w_in, w_gate, w_out, w_fg, w_fu, w_dn,
-    mix_gain, in_scale, gt_scale, conv_ref, recur_ref, ingate_ref, decay_ref, extra_ref,
-    out_scale, ffn_gain, fg_scale, fu_scale, dn_scale, out_ref,
-    W, X, N, BI, ST, GA, SB, RB, RB2, H, PS, F1, F2, F3, F4, F5, F6, F7, F8, MAP, RATES, EX,
-    send_sem, recv_sem, tp_send, tp_recv, own_sem,
+    recur_in, ingate_in, *rest,
 ):
+    small, out_ref, scratch = rest[:11], rest[11], rest[12:]
+    (
+        W, X, N, BI, ST, GA, SB, RB, RB2, H, PS, F1, F2, F3, F4, F5, F6, F7, F8, MAP, RATES, EX,
+    ) = scratch[:22]
+    kept = scratch[22:33]
+    (
+        mix_gain, in_scale, gt_scale, conv_ref, decay_ref, extra_ref, out_scale, ffn_gain,
+        fg_scale, fu_scale, dn_scale,
+    ) = kept
+    send_sem, recv_sem, tp_send, tp_recv, own_sem = scratch[33:]
     rep, fs, tp = lax.axis_index("rep"), lax.axis_index("fs"), lax.axis_index("tp")
     zl, y, x = fs // 16, (fs // 4) % 4, fs % 4
     rows, half = X.shape[1:]
@@ -137,7 +145,7 @@
     for i, (src, dst) in enumerate(
         [
             (w_in, F1), (tok, X.at[tp]), (w_gate, F2), (w_out, F3), (w_fg, F4), (w_fu, F5),
-            (w_dn, F6), (recur_ref, F7), (ingate_ref, F8),
+            (w_dn, F6), (recur_in, F7), (ingate_in, F8), *zip(small, kept),
         ]
     ):
         c = pltpu.make_async_copy(src, dst, own_sem.at[i])
@@ -221,30 +229,43 @@
         sizes = stage_bytes(width, last)
         return {s: v for s, v in steps.items() if s in sizes}
 
-    flights, landed = {}, set()
-
-    def land(k, s):
-        if (k, s) not in landed:
-            landed.add((k, s))
-            for c in flights[k, s]:
-                c.wait_recv()
+    issued, landed = set(), set()
+    stages = list(NEEDS)
+    rows_of_stage = dict(zip(stages, (64, 256, 128, 512, 512, 512, 64, 32, 256, 128, 512, 512, 512)))
+    arrive = dict(zip(stages, (0, 1, 2, 3, 4, 4, 5, 6, 7, 8, 9, 10, 10)))
+    depart = dict(zip(stages, (0, 1, 2, 3, 3, 4, 5, 6, 7, 8, 9, 9, 10)))
+
+    def whole_of(k, members):
+        start, width, last = chunks[k]
+        tail = members[0][0] == "c"
+        cols = pl.ds(start + width - last, last) if tail else pl.ds(start, width - last)
+        ref = {
+            32: (0, 0, 0, pl.ds(0, 32), cols), 64: (0, 0, 0, every, cols),
+            128: (0, 0, lo2, every, cols), 256: (0, 0, every, every, cols),
+            512: (0, lo2, every, every, cols), 1024: (0, every, every, every, cols),
+        }[sum(rows_of_stage[m] for m in members)]
+        return W.at[ref]
+
+    def wait_group(k, groups, g, arriving):
+        members = [m for m in stages if groups[m] == g and (k, m) in issued]
+        if members and (k, g, arriving) not in landed:
+            landed.add((k, g, arriving))
+            ref = whole_of(k, members)
+            c = remote(ref, ref, partner, send_sem.at[k, g], recv_sem.at[k, g])
+            c.wait_recv() if arriving else c.wait_send()
 
     def go(k, s):
-        steps = plan(k)
-        order = list(steps)
         for before in NEEDS[s]:
-            if before in steps:
-                land(k, before)
-        base = sum(len(steps[o]) for o in order[: order.index(s)])
-        flights[k, s] = []
-        for i, (ref, target) in enumerate(steps[s]):
-            c = remote(ref, ref, target, send_sem.at[k, base + i], recv_sem.at[k, base + i])
-            c.start()
-            flights[k, s].append(c)
+            wait_group(k, arrive, arrive[before], True)
+        issued.add((k, s))
+        for ref, target in plan(k)[s]:
+            remote(
+                ref, ref, target, send_sem.at[k, depart[s]], recv_sem.at[k, arrive[s]]
+            ).start()
 
     def done(k):
-        for s in plan(k):
-            land(k, s)
+        for g in range(11):
+            wait_group(k, arrive, g, True)
 
     def stage_weights(k):
         start = chunks[k][0]
@@ -275,8 +296,8 @@
 
     def prepare():
         zeros = jnp.zeros((64, 64), f32)
-        loads[6].wait()
-        loads[7].wait()
+        for c in loads[6:]:
+            c.wait()
         for g in range(half // LANES):
             for p in range(2):
                 r = F7[2 * g + p]
@@ -442,10 +463,10 @@
             cols = pl.ds(c, 256)
             scale = dn_scale[:, pl.ds(pl.multiple_of(tp * half + c, 256), 256)]
             total = PS[0, :, cols] + down(k, tp, j) + RB2[:, cols].astype(f32)
-            out_ref[:, cols] = (X[tp, :, cols].astype(f32) + total * scale).astype(bf16)
-            return carry
-
-        swaps = []
+            GA[:, cols] = (X[tp, :, cols].astype(f32) + total * scale).astype(bf16)
+            return carry
+
+        swaps, outs = [], []
         for i in range(2):
             lax.fori_loop(2 * i, 2 * i + 2, away, 0)
             cols = pl.ds(i * (half // 2), half // 2)
@@ -455,6 +476,12 @@
         for i in range(2):
             swaps[i].wait_recv()
             lax.fori_loop(2 * i, 2 * i + 2, home, 0)
+            cols = pl.ds(i * (half // 2), half // 2)
+            c = pltpu.make_async_copy(GA.at[:, cols], out_ref.at[:, cols], tp_recv.at[5 + i])
+            c.start()
+            outs.append(c)
+        for c in outs:
+            c.wait()
         for c in swaps:
             c.wait_send()
 
@@ -517,9 +544,9 @@
             compute(name)
         else:
             go(k, name)
-    for group in flights.values():
-        for c in group:
-            c.wait_send()
+    for k in range(n):
+        for g in range(11):
+            wait_group(k, depart, g, False)
 
 
 def local(*args):
@@ -538,13 +565,17 @@
     assert sum(TILES[6:]) == units
     n = len(chunks)
     row = lambda v: v[None, :]
-    vmem = pl.BlockSpec(memory_space=pltpu.VMEM)
+    small = (
+        row(mix_gain), row(lru_input_scale), row(lru_gate_scale), conv_weight, row(decay_rate),
+        row(extra_decay), row(lru_output_scale), row(ffn_gain), ffn_gate_scale, ffn_up_scale,
+        row(ffn_down_scale),
+    )
     hbm = pl.BlockSpec(memory_space=pl.ANY)
     return pl.pallas_call(
         functools.partial(layer_kernel, tuple(chunks)),
         out_shape=jax.ShapeDtypeStruct((rows, half), bf16),
-        in_specs=[hbm] * 7 + [vmem] * 4 + [hbm] * 2 + [vmem] * 7,
-        out_specs=vmem,
+        in_specs=[hbm] * 20,
+        out_specs=hbm,
         scratch_shapes=[
             pltpu.VMEM((2, 4, 4, 64, width), bf16),
             pltpu.VMEM((2, rows, half), bf16),
@@ -568,21 +599,20 @@
             pltpu.VMEM((half // LANES, LANES, 2 * LANES), f32),
             pltpu.VMEM((1, half), f32),
             pltpu.VMEM((rows, LANES), f32),
-            pltpu.SemaphoreType.DMA((n, 44)),
-            pltpu.SemaphoreType.DMA((n, 44)),
+            *(pltpu.VMEM(v.shape, f32) for v in small),
+            pltpu.SemaphoreType.DMA((n, 11)),
+            pltpu.SemaphoreType.DMA((n, 11)),
             pltpu.SemaphoreType.DMA((5,)),
-            pltpu.SemaphoreType.DMA((5,)),
-            pltpu.SemaphoreType.DMA((9,)),
+            pltpu.SemaphoreType.DMA((7,)),
+            pltpu.SemaphoreType.DMA((20,)),
         ],
         compiler_params=pltpu.CompilerParams(
-            collective_id=0, has_side_effects=True, vmem_limit_bytes=67043328
+            collective_id=0, has_side_effects=True, vmem_limit_bytes=VMEM
         ),
         name="layer",
     )(
-        tokens, lru_input, lru_gate, lru_output.T, ffn_gate, ffn_up, ffn_down.T, row(mix_gain),
-        row(lru_input_scale), row(lru_gate_scale), conv_weight, recur_gate, input_gate,
-        row(decay_rate), row(extra_decay), row(lru_output_scale), row(ffn_gain),
-        ffn_gate_scale, ffn_up_scale, row(ffn_down_scale),
+        tokens, lru_input, lru_gate, lru_output.T, ffn_gate, ffn_up, ffn_down.T, recur_gate,
+        input_gate, *small,
     )
 
 

time: 137 us -> 128 us (0.934)
  Pallas kernels: 134 us -> 126 us
    pallas_call x1, Pallas kernels: 134 us -> 126 us  [local(): pl.pallas_call(functools.partial(layer_kernel, tuple(chunks)), out_shape=...]
where the time goes in v3:
time: 128 us
  Pallas kernels  126 us (98%)
  local copies, waits for them, and re-layouts  2.26 us (2%)
    pallas_call x1, Pallas kernels, local(): pl.pallas_call(functools.partial(layer_kernel, tuple(chunks)), out_shape=...  126 us

profile of v3, /device:TPU:1, one launch (start us, length us, event | category | flops | bytes accessed | tf_op | source)
XLA Modules:
  0.0 128.3 jit_solution(15879347586437470494)
XLA Ops:
  0.0 126.0 %layer.1 = bf16[512,1024]{1,0:T(8,128)(2,1)} custom-call(bf16[512,1024]{1,0:T(8,128)(2,1)} %tok.1, f32[64,1024]{1,0:T(8,128)} %w_in.1, f32[64,1024]{1,0:T(8,128)} %w_gate.1, f32[64,1024]{1,0:T(8,128)} %bitcast.11, f32[64,1408]{1,0:T(8,128)} %w_fg.1, f32[64,1408]{1,0:T(8,128)} %w_fu.1, f32[64,1408]{1,0:T(8,128)} %bitcast.10, f32[16,64,64]{2,1,0:T(8,128)} %recur_in.1, ...), custom_call_target="tpu_custom_call" | custom-call | tf_op jit(solution)/shard_map/layer/pallas_call | solution.py:574
  126.0 2.3 %copy.22 = bf16[512,1024]{1,0:T(8,128)(2,1)} copy(bf16[512,1024]{1,0:T(8,128)(2,1)} %layer.1) | data formatting | bytes 2097152

commit v4 on v3

--- a/solution.py
+++ b/solution.py
@@ -17,22 +17,22 @@
     "c6": ("c5a",),
 }
 TILES = (8, 8, 8, 8, 8, 6, 8, 3)
-LAST = (3, 4, 7, 0, 4, 2, 1, 1)
-PRIORITY = (12.9, 0.9, 3.5, -7.5, 10.2, 10.3, -10.0, 3.7, -5.9, 2.9, 3.5, 7.4, 7.5)
+LAST = (0, 0, 1, 6, 3, 2, 3, 1)
+PRIORITY = (-7.1, -0.6, -10.7, 3.2, 3.9, -0.6, -8.8, -1.4, -4.4, -5.4, -2.1, -2.5, -3.7)
 VMEM = 67043328
-BACKLOG = 2.0
+BACKLOG = 5.0
 f32, bf16 = jnp.float32, jnp.bfloat16
 
 
 def stage_bytes(width, last):
     first, cut = width - last, (last // LANES + 1) // 2 * LANES
     plane = lambda r, w: {d: r * w for d in range(4)}
-    depth = lambda r, w: {d: r * w for d in (4, 5)}
     sizes = {
-        "z0": depth(32, first), "s1": plane(64, first), "s2": plane(32, first),
+        "z0": {5: 64 * first}, "s1": plane(64, first), "s2": plane(32, first),
         "s3a": plane(128, first), "s3b": plane(128, first), "s4": plane(128, first),
         "c1": plane(16, last), "c2": plane(16, cut), "c3": plane(64, last), "c4": plane(32, last),
-        "c5a": depth(256, last), "c5b": depth(256, last), "c6": depth(256, last),
+        "c5a": {4: 384 * last, 5: 128 * last}, "c5b": {4: 128 * last, 5: 384 * last},
+        "c6": {4: 128 * last, 5: 384 * last},
     }
     return {s: v for s, v in sizes.items() if sum(v.values()) > 0}
 
@@ -43,17 +43,18 @@
     free, land, staged, ended = [0.0] * 6, {}, [None] * count, {}
     todo = [(k, s) for k in range(count) for s in sizes[k]]
     todo.sort(key=lambda c: (c[0] + PRIORITY[steps.index(c[1])], steps.index(c[1])))
+    todo = [(-2, i) for i in range(PIECES)] + todo
     order, now, work, never = [], 0.0, list(work), 1e9
+    token_piece = {4: 512 * 1024 // PIECES}
     whole = lambda k: max(land.get((k, s), never) for s in sizes[k])
     while todo or work:
         pick, later = None, never
         for k, s in todo:
-            if staged[k] is None:
+            if staged[max(k, 0)] is None:
                 continue
-            ready = max(
-                [staged[k]] + [land.get((k, d), never) for d in NEEDS[s] if d in sizes[k]]
-            )
-            queue = max(free[d] for d in sizes[k][s]) - now
+            before = () if k < 0 else [d for d in NEEDS[s] if d in sizes[k]]
+            ready = max([staged[max(k, 0)]] + [land.get((k, d), never) for d in before])
+            queue = max(free[d] for d in (token_piece if k < 0 else sizes[k][s])) - now
             if ready > now:
                 later = min(later, ready)
             elif queue > BACKLOG:
@@ -65,15 +66,18 @@
             k, s = pick
             todo.remove(pick)
             order.append(pick)
-            for d, size in sizes[k][s].items():
+            parts = token_piece if k < 0 else sizes[k][s]
+            for d, size in parts.items():
                 free[d] = max(free[d], now) + size * 2 / rate
-            land[pick] = max(free[d] for d in sizes[k][s]) + latency
+            land[pick] = max(free[d] for d in parts) + latency
+            if k < 0:
+                ended["tokens"] = land[pick] if s == PIECES - 1 else never
             now += 0.15
             continue
         if work:
             name, cost, reads, after = work[0]
             ready = max(
-                [0.0] + [whole(k) for k in reads] + [ended[w] + delay for w, delay in after]
+                [0.0] + [whole(k) for k in reads] + [ended.get(w, never) + delay for w, delay in after]
             )
             if ready <= now:
                 work.pop(0)
@@ -82,6 +86,9 @@
                 ended[name] = now
                 if name[:5] == "stage":
                     staged[int(name[5:])] = now
+                if name in SENDS:
+                    free[4] = max(free[4], now) + SENDS[name] * 2 / rate
+                    ended["sent" + name] = free[4] + latency
                 continue
             if ready < never:
                 later = min(later, ready)
@@ -89,12 +96,16 @@
     return order
 
 
+PIECES = 8
+SENDS = {"gate0": 512 * 512}
 WORK = (
     tuple((f"stage{k}", 0.35, (), ()) for k in range(len(TILES)))
-    + (("prep", 1.0, (), ()), ("norm1", 1.1, (), ()), ("in", 2.8, (0,), ()))
+    + (("prep", 1.0, (), ()), ("norm1", 1.1, (), ()),
+       ("ptok", 0.2, (), (("tokens", 0.0),)), ("in1", 1.4, (0,), ()),
+       ("norm1p", 1.1, (), (("ptok", 3.2),)), ("in0", 1.4, (), ()))
     + tuple((f"scan{i}", 2.4, (), ()) for i in range(4))
     + (
-        ("gate0", 1.7, (1,), ()), ("gate1", 1.7, (), ()), ("outA", 1.6, (2,), ()),
+        ("gate0", 1.7, (1,), ()), ("gate1", 1.7, (), ()), ("outA", 1.6, (2,), (("sentgate0", 0.0),)),
         ("outH", 1.6, (), ()), ("mixed", 0.8, (), (("outA", 3.0),)),
         ("norm2", 1.1, (), (("mixed", 3.2),)), ("hid0", 2.9, (3,), ()), ("hid1", 2.9, (4,), ()),
         ("hid2", 2.2, (5,), ()), ("downA", 1.8, (6,), ()), ("downH", 1.8, (), ()),
@@ -114,13 +125,14 @@
     small, out_ref, scratch = rest[:11], rest[11], rest[12:]
     (
         W, X, N, BI, ST, GA, SB, RB, RB2, H, PS, F1, F2, F3, F4, F5, F6, F7, F8, MAP, RATES, EX,
-    ) = scratch[:22]
-    kept = scratch[22:33]
+        XP, NP, GP, EP,
+    ) = scratch[:26]
+    kept = scratch[26:37]
     (
         mix_gain, in_scale, gt_scale, conv_ref, decay_ref, extra_ref, out_scale, ffn_gain,
         fg_scale, fu_scale, dn_scale,
     ) = kept
-    send_sem, recv_sem, tp_send, tp_recv, own_sem = scratch[33:]
+    send_sem, recv_sem, tp_send, tp_recv, own_sem = scratch[37:]
     rep, fs, tp = lax.axis_index("rep"), lax.axis_index("fs"), lax.axis_index("tp")
     zl, y, x = fs // 16, (fs // 4) % 4, fs % 4
     rows, half = X.shape[1:]
@@ -132,13 +144,11 @@
     to_x = lambda v: (rep, zl * 16 + y * 4 + v, tp)
     to_y = lambda v: (rep, zl * 16 + v * 4 + x, tp)
     z_other = away_zl * 16 + y * 4 + x
-    rep_next = jnp.where(zl == 0, rep, 1 - rep)
-    rep_prev = 1 - rep_next
-    z_next, z_prev = (rep_next, z_other, tp), (rep_prev, z_other, tp)
+    pair, apart = (rep, z_other, tp), (1 - rep, z_other, tp)
     partner = (rep, fs, other)
 
     barrier = pltpu.get_barrier_semaphore()
-    for peer in (to_x(xl), to_x(xr), to_y(yl), to_y(yr), z_next, z_prev, partner):
+    for peer in (to_x(xl), to_x(xr), to_y(yl), to_y(yr), pair, apart, partner):
         pl.semaphore_signal(barrier, inc=1, device_id=peer, device_id_type=MESH)
 
     loads = []
@@ -165,8 +175,9 @@
     mine_rows = pl.ds(pl.multiple_of(rep * 32, 32), 32)
     CA = pl.ds(pl.multiple_of(rep * 32, 16), 16)
     CB = pl.ds(pl.multiple_of(rep * 32 + 16, 16), 16)
-    next_rows = pl.ds(pl.multiple_of(rep_next * 32, 32), 32)
-    prev_rows = pl.ds(pl.multiple_of(rep_prev * 32, 32), 32)
+    far_rows = pl.ds(pl.multiple_of((1 - rep) * 32, 32), 32)
+    part = half // 2
+    own_part, pair_part = pl.multiple_of(zl * part, part), pl.multiple_of(away_zl * part, part)
     up_x, dn_x, up_y, dn_y = to_x(xr), to_x(xl), to_y(yr), to_y(yl)
     def plan(k):
         start, width, last = chunks[k]
@@ -174,10 +185,13 @@
         cut = (last // LANES + 1) // 2 * LANES
         t1 = pl.ds(start + width - last, cut)
         t2 = pl.ds(start + width - last + cut, last - cut)
+        if k < 2:
+            cols = pl.ds(start + own_part, width)
+        sent = pl.ds(start + pair_part, width) if k < 2 else cols
         at = lambda a, b, c, r: W.at[a, b, c, r, cols]
         ct = lambda a, b, c, r, t=tail: W.at[a, b, c, r, t] if t.size else None
         steps = {
-            "z0": [(at(zl, y, x, A), z_next), (at(zl, y, x, B), z_prev)],
+            "z0": [(W.at[zl, y, x, :, sent], apart)],
             "s1": [
                 (at(every, y, x, A), up_x), (at(every, y, x, A), dn_x),
                 (at(every, y, x, B), up_y), (at(every, y, x, B), dn_y),
@@ -215,14 +229,16 @@
                 (ct(zl, lo2, xl, CB), up_x), (ct(zl, hi2, xr, CB), dn_x),
             ],
             "c5a": [
-                (ct(zl, lo2, every, mine_rows), z_next), (ct(zl, hi2, every, mine_rows), z_prev),
+                *((ct(zl, j, every, mine_rows), pair) for j in (1, 2, 3)),
+                (ct(zl, 0, every, mine_rows), apart),
             ],
             "c5b": [
-                (ct(zl, hi2, every, mine_rows), z_next), (ct(zl, lo2, every, mine_rows), z_prev),
+                (ct(zl, 0, every, mine_rows), pair),
+                *((ct(zl, j, every, mine_rows), apart) for j in (1, 2, 3)),
             ],
             "c6": [
-                (ct(away_zl, lo2, every, prev_rows), z_next),
-                (ct(away_zl, hi2, every, next_rows), z_prev),
+                (ct(away_zl, 0, every, far_rows), pair),
+                *((ct(away_zl, j, every, mine_rows), apart) for j in (1, 2, 3)),
             ],
         }
         steps["c2"] = steps["c2"] if last > cut else steps["c2"][::2]
@@ -296,7 +312,7 @@
 
     def prepare():
         zeros = jnp.zeros((64, 64), f32)
-        for c in loads[6:]:
+        for c in loads[6:13] + loads[14:]:
             c.wait()
         for g in range(half // LANES):
             for p in range(2):
@@ -306,9 +322,9 @@
                 MAP[g, p * 64 : p * 64 + 64, :] = jnp.concatenate(parts, axis=1)
         v = -decay_ref[...]
         RATES[...] = -RATE * (jnp.maximum(v, 0.0) + jnp.log1p(jnp.exp(-jnp.abs(v))))
-        EX[...] = jnp.broadcast_to(extra_ref[...], (LANES, rows)).T
-
-    def norm_rows(gain):
+        EX[1] = jnp.broadcast_to(extra_ref[...], (LANES, rows)).T
+
+    def norm_rows(X, N, gain):
         step = 64
 
         def body(i, carry):
@@ -333,21 +349,23 @@
     def dot_t(a, b):
         return lax.dot_general(a, b, (((1,), (1,)), ((), ())), preferred_element_type=f32)
 
-    def branch_in():
+    def branch_in(seq):
         def body(i, carry):
             c = pl.multiple_of(i * 256, 256)
-            BI[:, pl.ds(c, 256)] = (
-                dot(N[...], wide(c, 256)) * in_scale[:, pl.ds(c, 256)]
+            g = pl.multiple_of(own_part + c, 256)
+            BI[seq, :, pl.ds(c, 256)] = (
+                dot((NP, N)[seq][...], wide(g, 256)) * in_scale[:, pl.ds(g, 256)]
             ).astype(bf16)
             return carry
 
-        lax.fori_loop(0, half // 256, body, 0)
-
-    def scan_block(i, carry):
-        cols = pl.ds(pl.multiple_of(i * LANES, LANES), LANES)
+        lax.fori_loop(0, part // 256, body, 0)
+
+    def scan_block(seq, i, carry):
+        held = pl.ds(pl.multiple_of(i * LANES, LANES), LANES)
+        cols = pl.ds(pl.multiple_of(own_part + i * LANES, LANES), LANES)
         length = rows
         taps = conv_ref.shape[0]
-        values = BI[:, cols].astype(f32)
+        values = BI[seq, :, held].astype(f32)
         weights = conv_ref[:, cols]
         row = lax.broadcasted_iota(jnp.int32, values.shape, 0)
         conv = weights[taps - 1 : taps, :] * values
@@ -355,11 +373,11 @@
             moved = jnp.where(row >= back, pltpu.roll(values, back, 0), 0.0)
             conv = conv + weights[taps - 1 - back : taps - back, :] * moved
         mapped = jnp.dot(
-            conv, MAP[i], preferred_element_type=f32, precision=lax.Precision.HIGHEST
+            conv, MAP[zl * (part // LANES) + i], preferred_element_type=f32, precision=lax.Precision.HIGHEST
         )
         recur = sigmoid(mapped[:, :LANES])
         ingate = sigmoid(mapped[:, LANES:])
-        log_rate = RATES[:, cols] * recur - EX[...]
+        log_rate = RATES[:, cols] * recur - EX[seq]
         a = jnp.exp(log_rate)
         u = -2.0 * log_rate
         series = u * (1 - u / 2 * (1 - u / 3 * (1 - u / 4 * (1 - u / 5 * (1 - u / 6)))))
@@ -381,16 +399,23 @@
             cb = jnp.concatenate([cb[:s], cb_new], axis=0)
             ca = jnp.concatenate([ca[:s], ca_new], axis=0)
             s *= 2
-        ST[:, cols] = jnp.concatenate([b[:8], a[8:] * cb[:-8] + b[8:]], axis=0)
+        ST[seq, :, held] = jnp.concatenate([b[:8], a[8:] * cb[:-8] + b[8:]], axis=0)
         return carry
 
-    def gate_block(i, carry):
+    def gate_block(seq, i, carry):
         c = pl.multiple_of(i * 256, 256)
-        cols = pl.ds(c, 256)
-        acc = dot(N[...], wide(pl.multiple_of(half + c, 256), 256)) * gt_scale[:, cols]
-        g = acc.astype(bf16).astype(f32)
-        gelu = 0.5 * g * (1.0 + jnp.tanh(0.7978845608028654 * (g + 0.044715 * g * g * g)))
-        GA[:, cols] = (ST[:, cols] * gelu).astype(bf16)
+        g = pl.multiple_of(own_part + c, 256)
+        scale = gt_scale[:, pl.ds(g, 256)]
+        acc = dot((NP, N)[seq][...], wide(pl.multiple_of(half + g, 256), 256)) * scale
+        g16 = acc.astype(bf16).astype(f32)
+        gelu = 0.5 * g16 * (
+            1.0 + jnp.tanh(0.7978845608028654 * (g16 + 0.044715 * g16 * g16 * g16))
+        )
+        gated = (ST[seq, :, pl.ds(c, 256)] * gelu).astype(bf16)
+        if seq == 0:
+            GP[:, pl.ds(c, 256)] = gated
+        else:
+            GA[:, pl.ds(g, 256)] = gated
         return carry
 
     def rows_of(block, j, start, width):
@@ -486,6 +511,12 @@
             c.wait_send()
 
     swap_tok = remote(X.at[tp], X.at[tp], partner, tp_send.at[0], tp_recv.at[0])
+    swap_pair = remote(X.at[tp], XP.at[tp], pair, tp_send.at[5], tp_recv.at[7])
+    swap_ptok = remote(XP.at[tp], XP.at[tp], partner, tp_send.at[6], tp_recv.at[8])
+    swap_extra = remote(extra_ref, EP, pair, tp_send.at[7], tp_recv.at[9])
+    swap_gated = remote(
+        GP, GA.at[:, pl.ds(own_part, part)], pair, tp_send.at[8], tp_recv.at[10]
+    )
     swap_out = remote(SB, RB, partner, tp_send.at[1], tp_recv.at[1])
     swap_mix = remote(X.at[tp], X.at[tp], partner, tp_send.at[2], tp_recv.at[2])
 
@@ -493,28 +524,42 @@
         if name == "stage0":
             stage_weights(0)
             pl.semaphore_wait(barrier, 7)
+            loads[13].wait()
+            swap_extra.start()
+            keep.wait()
+            swap_tok.start()
         elif name[:5] == "stage":
             stage_weights(int(name[5:]))
-            if name == "stage1":
-                keep.wait()
-                swap_tok.start()
         elif name == "prep":
             prepare()
         elif name == "norm1":
             swap_tok.wait()
-            norm_rows(mix_gain)
-        elif name == "in":
+            norm_rows(X, N, mix_gain)
+        elif name == "ptok":
+            swap_pair.wait()
+            swap_ptok.start()
+        elif name == "norm1p":
+            swap_ptok.wait()
+            swap_extra.wait()
+            EX[0] = jnp.broadcast_to(EP[...], (LANES, rows)).T
+            norm_rows(XP, NP, mix_gain)
+        elif name[:2] == "in":
             done(0)
-            branch_in()
+            branch_in(int(name[2:]))
         elif name[:4] == "scan":
             i = int(name[4:])
-            lax.fori_loop(2 * i, 2 * i + 2, scan_block, 0)
+            first = 2 * (i % 2)
+            scan = functools.partial(scan_block, i // 2)
+            lax.fori_loop(first, first + 2, scan, 0)
         elif name[:4] == "gate":
             done(1)
             i = int(name[4:])
-            lax.fori_loop(2 * i, 2 * i + 2, gate_block, 0)
+            lax.fori_loop(0, 2, functools.partial(gate_block, i), 0)
+            if i == 0:
+                swap_gated.start()
         elif name == "outA":
             done(2)
+            swap_gated.wait()
             out_away()
             swap_out.start()
         elif name == "outH":
@@ -525,7 +570,7 @@
             swap_mix.start()
         elif name == "norm2":
             swap_mix.wait()
-            norm_rows(ffn_gain)
+            norm_rows(X, N, ffn_gain)
         elif name[:3] == "hid":
             k = 3 + int(name[3:])
             done(k)
@@ -540,7 +585,12 @@
             finish(7)
 
     for k, name in arrange(chunks, WORK):
-        if k < 0:
+        if k == -2:
+            part_rows = pl.ds(name * (rows // PIECES), rows // PIECES)
+            remote(
+                X.at[tp, part_rows], XP.at[tp, part_rows], pair, tp_send.at[5], tp_recv.at[7]
+            ).start()
+        elif k < 0:
             compute(name)
         else:
             go(k, name)
@@ -558,8 +608,8 @@
     rows, half = tokens.shape
     units = ffn_gate.shape[1] // LANES
     chunks, width = [], 0
-    for tiles, last in zip(TILES, LAST):
-        chunks.append((width, tiles * LANES, last * LANES))
+    for k, (tiles, last) in enumerate(zip(TILES, LAST)):
+        chunks.append((width, (tiles // 2 if k < 2 else tiles) * LANES, last * LANES))
         width += tiles * LANES
     assert sum(TILES[:3]) * LANES == 3 * half and sum(TILES[3:6]) == 2 * units
     assert sum(TILES[6:]) == units
@@ -580,8 +630,8 @@
             pltpu.VMEM((2, 4, 4, 64, width), bf16),
             pltpu.VMEM((2, rows, half), bf16),
             pltpu.VMEM((rows, 2 * half), bf16),
-            pltpu.VMEM((rows, half), bf16),
-            pltpu.VMEM((rows, half), f32),
+            pltpu.VMEM((2, rows, half // 2), bf16),
+            pltpu.VMEM((2, rows, half // 2), f32),
             pltpu.VMEM((rows, half), bf16),
             pltpu.VMEM((rows, half), bf16),
             pltpu.VMEM((rows, half), bf16),
@@ -598,12 +648,16 @@
             pltpu.VMEM(input_gate.shape, f32),
             pltpu.VMEM((half // LANES, LANES, 2 * LANES), f32),
             pltpu.VMEM((1, half), f32),
-            pltpu.VMEM((rows, LANES), f32),
+            pltpu.VMEM((2, rows, LANES), f32),
+            pltpu.VMEM((2, rows, half), bf16),
+            pltpu.VMEM((rows, 2 * half), bf16),
+            pltpu.VMEM((rows, half // 2), bf16),
+            pltpu.VMEM((1, rows), f32),
             *(pltpu.VMEM(v.shape, f32) for v in small),
             pltpu.SemaphoreType.DMA((n, 11)),
             pltpu.SemaphoreType.DMA((n, 11)),
-            pltpu.SemaphoreType.DMA((5,)),
-            pltpu.SemaphoreType.DMA((7,)),
+            pltpu.SemaphoreType.DMA((9,)),
+            pltpu.SemaphoreType.DMA((11,)),
             pltpu.SemaphoreType.DMA((20,)),
         ],
         compiler_params=pltpu.CompilerParams(

time: 128 us -> 122 us (0.953)
  Pallas kernels: 126 us -> 119 us
    pallas_call x1, Pallas kernels: 126 us -> 119 us  [local(): pl.pallas_call(functools.partial(layer_kernel, tuple(chunks)), out_shape=...]
where the time goes in v4:
time: 122 us; the launch traced here: 121 us
  Pallas kernels  119 us (98%)
  local copies, waits for them, and re-layouts  2.26 us (2%)
    pallas_call x1, Pallas kernels, local(): pl.pallas_call(functools.partial(layer_kernel, tuple(chunks)), out_shape=...  119 us

profile of v4, /device:TPU:1, one launch (start us, length us, event | category | flops | bytes accessed | tf_op | source)
XLA Modules:
  0.0 121.4 jit_solution(13690135686733225312)
XLA Ops:
  0.0 119.1 %layer.1 = bf16[512,1024]{1,0:T(8,128)(2,1)} custom-call(bf16[512,1024]{1,0:T(8,128)(2,1)} %tok.1, f32[64,1024]{1,0:T(8,128)} %w_in.1, f32[64,1024]{1,0:T(8,128)} %w_gate.1, f32[64,1024]{1,0:T(8,128)} %bitcast.11, f32[64,1408]{1,0:T(8,128)} %w_fg.1, f32[64,1408]{1,0:T(8,128)} %w_fu.1, f32[64,1408]{1,0:T(8,128)} %bitcast.10, f32[16,64,64]{2,1,0:T(8,128)} %recur_in.1, ...), custom_call_target="tpu_custom_call" | custom-call | tf_op jit(solution)/shard_map/layer/pallas_call | solution.py:624
  119.2 2.3 %copy.22 = bf16[512,1024]{1,0:T(8,128)(2,1)} copy(bf16[512,1024]{1,0:T(8,128)(2,1)} %layer.1) | data formatting | bytes 2097152

commit v5 on v4

--- a/solution.py
+++ b/solution.py
@@ -17,10 +17,10 @@
     "c6": ("c5a",),
 }
 TILES = (8, 8, 8, 8, 8, 6, 8, 3)
-LAST = (0, 0, 1, 6, 3, 2, 3, 1)
-PRIORITY = (-7.1, -0.6, -10.7, 3.2, 3.9, -0.6, -8.8, -1.4, -4.4, -5.4, -2.1, -2.5, -3.7)
+LAST = (0, 0, 3, 6, 3, 2, 1, 1)
+PRIORITY = (-1.7, 2.7, -0.4, 5.3, 7.4, -16.7, -1.9, -0.9, -5.2, -12.8, -7.4, -8.0, -17.8)
 VMEM = 67043328
-BACKLOG = 5.0
+BACKLOG = 5
 f32, bf16 = jnp.float32, jnp.bfloat16
 
 

time: 122 us -> 121 us (level)
  no operation moved by 1% of the time
where the time goes in v5:
time: 121 us
  Pallas kernels  118 us (98%)
  local copies, waits for them, and re-layouts  2.26 us (2%)
    pallas_call x1, Pallas kernels, local(): pl.pallas_call(functools.partial(layer_kernel, tuple(chunks)), out_shape=...  118 us

profile of v5, /device:TPU:1, one launch (start us, length us, event | category | flops | bytes accessed | tf_op | source)
XLA Modules:
  0.0 120.7 jit_solution(3759554850287658582)
XLA Ops:
  0.0 118.4 %layer.1 = bf16[512,1024]{1,0:T(8,128)(2,1)} custom-call(bf16[512,1024]{1,0:T(8,128)(2,1)} %tok.1, f32[64,1024]{1,0:T(8,128)} %w_in.1, f32[64,1024]{1,0:T(8,128)} %w_gate.1, f32[64,1024]{1,0:T(8,128)} %bitcast.11, f32[64,1408]{1,0:T(8,128)} %w_fg.1, f32[64,1408]{1,0:T(8,128)} %w_fu.1, f32[64,1408]{1,0:T(8,128)} %bitcast.10, f32[16,64,64]{2,1,0:T(8,128)} %recur_in.1, ...), custom_call_target="tpu_custom_call" | custom-call | tf_op jit(solution)/shard_map/layer/pallas_call | solution.py:624
  118.5 2.3 %copy.22 = bf16[512,1024]{1,0:T(8,128)(2,1)} copy(bf16[512,1024]{1,0:T(8,128)(2,1)} %layer.1) | data formatting | bytes 2097152
